TPU v7x, 32 devices: a whole 2x2x4 slice. The times are simulated.
32 devices in a mesh: fs: 8 (over z, core), tp: 4 (over y, x).
Axes of the slice: x: 2, y: 2, z: 4, core: 2. Of those that a mesh axis runs over, the one named last changes fastest.
Arguments:
- rows_later: bfloat16 [6144, 2048], P('fs'), may hold values from -6 to 6
- rows_earlier: bfloat16 [6144, 2048], P('fs'), may hold values from -6 to 6
- out_cotangent: bfloat16 [6144, 4096], P('fs', 'tp'), may hold values from -6 to 6
- gate_proj: bfloat16 [2048, 4096], P('fs', 'tp'), may hold values from -0.125 to 0.125
- up_proj: bfloat16 [2048, 4096], P('fs', 'tp'), may hold values from -0.125 to 0.125
- conv_taps: float32 [3, 4096], P(None, 'tp'), may hold values from -4 to 4
- conv_bias: float32 [4096], P('tp'), may hold values from -3 to 3
- gate_grad_sum: float32 [2048, 4096], P('fs', 'tp'), may hold values from -6 to 6
- up_grad_sum: float32 [2048, 4096], P('fs', 'tp'), may hold values from -6 to 6
- taps_grad_sum: float32 [3, 4096], P(None, 'tp'), may hold values from -6 to 6
- bias_grad_sum: float32 [4096], P('tp'), may hold values from -6 to 6
Outputs:
- hidden_later: bfloat16 [6144, 4096], P('fs', 'tp')
- input_grad: bfloat16 [6144, 2048], P('fs')
- gate_grad_out: float32 [2048, 4096], P('fs', 'tp')
- up_grad_out: float32 [2048, 4096], P('fs', 'tp')
- taps_grad_out: float32 [3, 4096], P(None, 'tp')
- bias_grad_out: float32 [4096], P('tp')
All inputs are finite; a program needn't handle non-finite values.
Results may differ from a plain program's by a relative error of at most 0.019.
Values may be sent and summed in bfloat16 or wider, within the bound.
A program may use at most 128 MiB of HBM per device.

v0:
```python
import jax
import jax.numpy as jnp
from jax import lax
from jax.sharding import PartitionSpec as P


def shift_down(values, distance):
    total_len = values.shape[1]
    return jnp.pad(values, ((0, 0), (distance, 0), (0, 0)))[:, :total_len]


def shift_up(values, distance):
    return jnp.pad(values, ((0, 0), (0, distance), (0, 0)))[:, distance:]


def causal_mix(pre_values, conv_taps, conv_bias):
    return (
        conv_taps[0] * shift_down(pre_values, 2)
        + conv_taps[1] * shift_down(pre_values, 1)
        + conv_taps[2] * pre_values
        + conv_bias
    )


def mix_adjoint(mixed_grad, conv_taps):
    return (
        conv_taps[2] * mixed_grad
        + conv_taps[1] * shift_up(mixed_grad, 1)
        + conv_taps[0] * shift_up(mixed_grad, 2)
    )


def contract_last(left, right):
    return lax.dot_general(
        left, right, (((1,), (1,)), ((), ())), preferred_element_type=jnp.float32
    )


def contract_first(left, right):
    return lax.dot_general(
        left, right, (((0,), (0,)), ((), ())), preferred_element_type=jnp.float32
    )


def on_device(
    rows_later,
    rows_earlier,
    out_cotangent,
    gate_proj,
    up_proj,
    conv_taps,
    conv_bias,
    gate_grad_sum,
    up_grad_sum,
    taps_grad_sum,
    bias_grad_sum,
):
    seq_len = rows_later.shape[0]
    shard_width = out_cotangent.shape[1]
    stacked_rows = jnp.concatenate([rows_later, rows_earlier], axis=0)
    paired = jnp.stack([gate_proj, up_proj], axis=0)
    pieces = lax.all_gather(paired, "fs", axis=1, tiled=True)
    gate_acc = jnp.dot(stacked_rows, pieces[0], preferred_element_type=jnp.float32)
    up_acc = jnp.dot(stacked_rows, pieces[1], preferred_element_type=jnp.float32)
    gate_pre = gate_acc.astype(jnp.bfloat16)
    up_value = up_acc.astype(jnp.bfloat16)
    gate_pre, up_value = lax.optimization_barrier((gate_pre, up_value))
    gate_float = gate_pre.astype(jnp.float32).reshape(2, seq_len, shard_width)
    up_float = up_value.astype(jnp.float32).reshape(2, seq_len, shard_width)
    mixed = causal_mix(gate_float, conv_taps, conv_bias)
    sig_all = jax.nn.sigmoid(mixed)
    activated = mixed * sig_all
    hidden = (activated * up_float).astype(jnp.bfloat16)
    hidden_later = hidden[0]
    grad_scale = lax.rsqrt(jnp.asarray(seq_len * lax.axis_size("fs"), jnp.float32))

    def make_term(grad_rows):
        return contract_first(rows_earlier, grad_rows)

    cotangent = out_cotangent.astype(jnp.float32)[None]
    mixed_back = mixed[1:]
    sig_back = sig_all[1:]
    up_grad = (cotangent * activated[1:]).astype(jnp.bfloat16)[0]
    up_summed = lax.psum_scatter(
        make_term(up_grad).astype(jnp.bfloat16), "fs", scatter_dimension=0, tiled=True
    ).astype(jnp.float32)
    mixed_grad = cotangent * up_float[1:] * sig_back * (1.0 + mixed_back * (1.0 - sig_back))
    gate_grad = mix_adjoint(mixed_grad, conv_taps).astype(jnp.bfloat16)[0]
    gate_summed = lax.psum_scatter(
        make_term(gate_grad).astype(jnp.bfloat16), "fs", scatter_dimension=0, tiled=True
    ).astype(jnp.float32)
    pieces = lax.all_gather(paired, "fs", axis=1, tiled=True)
    partial_rows = contract_last(gate_grad, pieces[0]) + contract_last(up_grad, pieces[1])
    input_grad = lax.psum(partial_rows.astype(jnp.bfloat16), "tp")
    gate_grad_out = gate_grad_sum + grad_scale * gate_summed
    up_grad_out = up_grad_sum + grad_scale * up_summed
    gate_back = gate_float[1:]
    tap_local = jnp.stack(
        [
            jnp.sum(mixed_grad * shift_down(gate_back, 2 - tap_index), axis=(0, 1))
            for tap_index in range(conv_taps.shape[0])
        ]
    )
    bias_local = jnp.sum(mixed_grad, axis=(0, 1))
    tap_total, bias_total = lax.psum((tap_local, bias_local), "fs")
    taps_grad_out = taps_grad_sum + grad_scale * tap_total
    bias_grad_out = bias_grad_sum + grad_scale * bias_total
    return (hidden_later, input_grad, gate_grad_out, up_grad_out, taps_grad_out, bias_grad_out)


def solution(mesh):
    placed = (
        P("fs", None),
        P("fs", None),
        P("fs", "tp"),
        P("fs", "tp"),
        P("fs", "tp"),
        P(None, "tp"),
        P("tp"),
        P("fs", "tp"),
        P("fs", "tp"),
        P(None, "tp"),
        P("tp"),
    )
    return jax.shard_map(
        on_device,
        mesh=mesh,
        in_specs=placed,
        out_specs=(
            P("fs", "tp"),
            P("fs", None),
            P("fs", "tp"),
            P("fs", "tp"),
            P(None, "tp"),
            P("tp"),
        ),
        check_vma=False,
    )
```

profile of v0, /device:TPU:16, one launch (start us, length us, event | category | flops | bytes accessed | tf_op | source)
XLA Modules:
  0.0 332.2 jit_solution(14247439538161545756)
XLA Ops:
  7.2 2.4 pad_maximum_fusion
  9.7 0.9 fusion.32
  10.7 2.0 constant_dynamic-update-slice_fusion.1
  12.6 2.1 constant_dynamic-update-slice_fusion
  14.8 77.0 %all-gather.2.cloned.1.call-done = bf16[2,2048,1024]{2,1,0:T(8,128)(2,1)} async-done(((bf16[2,256,1024]{2,1,0:T(8,128)(2,1)}), bf16[2,2048,1024]{2,1,0:T(8,128)(2,1)}) %all-gather.2.cloned.1.call-update) | async-done | bytes 8388624 | tf_op jit(solution)/shard_map/all_gather | solution.py:62
  91.8 10.1 %convolution_convert_fusion = bf16[1536,1024]{1,0:T(8,128)(2,1)S(1)} fusion(bf16[1536,2048]{1,0:T(8,128)(2,1)} %constant_dynamic-update-slice_fusion, bf16[2,2048,1024]{2,1,0:T(8,128)(2,1)} %all-gather.2.cloned.1.call-done), kind=kOutput, calls=%fused_computation.15 | convolution fusion | flops 6444023808 | bytes 13631488 | tf_op jit(solution)/shard_map/dot_general | solution.py:64
  102.0 8.8 %convolution_convert_fusion.1 = bf16[1536,1024]{1,0:T(8,128)(2,1)S(1)} fusion(bf16[1536,2048]{1,0:T(8,128)(2,1)} %constant_dynamic-update-slice_fusion, bf16[2,2048,1024]{2,1,0:T(8,128)(2,1)S(1)} %copy-done.15), kind=kOutput, calls=%fused_computation.16 | convolution fusion | flops 6444023808 | bytes 13631488 | tf_op jit(solution)/shard_map/dot_general | solution.py:63
  110.8 0.7 convert_element_type.59
  111.5 1.9 slice_bitcast_fusion.6
  113.4 0.7 convert_element_type.60
  114.1 3.2 add_divide_fusion
  117.9 6.3 %fusion.13 = (f32[1024]{0:T(1024)S(1)}, f32[1024]{0:T(1024)S(1)}, f32[1024]{0:T(1024)S(1)}, f32[1024]{0:T(1024)S(1)}, f32[1,768,1024]{2,1,0:T(8,128)S(1)}) fusion(f32[1,768,1024]{2,1,0:T(8,128)} %slice_bitcast_fusion.6, f32[1536,1024]{1,0:T(8,128)S(1)} %convert_element_type.59, f32[2,768,1024]{2,1,0:T(8,128)S(1)} %get-tuple-element.24, ...), kind=kLoop, calls=%fused_computation.29 | loop fusion | flops 11005952 | bytes 20463616 | tf_op jit(solution)/shard_map/reduce_sum | solution.py:100
  124.3 1.0 fusion.10
  125.3 1.1 copy-done.9
  126.4 5.1 %convert_bitcast_fusion.1 = bf16[2048,1024]{0,1:T(8,128)(2,1)} fusion(bf16[768,2048]{1,0:T(8,128)(2,1)S(1)} %copy-done.6, bf16[1,768,1024]{2,1,0:T(8,128)(2,1)S(1)} %fusion.10), kind=kOutput, calls=%fused_computation.12 | convolution fusion | flops 3223322624 | bytes 8912896 | tf_op jit(solution)/shard_map/dot_general | solution.py:40
  131.7 4.5 %fusion.29 = f32[2,768,1024]{2,1,0:T(8,128)S(1)} fusion(f32[2,768,1024]{2,1,0:T(8,128)} %copy-done), kind=kLoop, calls=%fused_computation.55 | loop fusion | flops 6291456 | bytes 12582912 | tf_op jit(solution)/shard_map/mul | solution.py:72
  136.3 2.6 copy-done.2
  138.8 5.1 %convert_bitcast_fusion = bf16[2048,1024]{0,1:T(8,128)(2,1)} fusion(bf16[768,2048]{1,0:T(8,128)(2,1)S(1)} %copy-done.6, f32[2,768,1024]{2,1,0:T(8,128)S(1)} %fusion.29, bf16[768,1024]{1,0:T(8,128)(2,1)S(1)} %copy-done.7), kind=kOutput, calls=%fused_computation.11 | convolution fusion | flops 3225681920 | bytes 12058624 | tf_op jit(solution)/shard_map/dot_general | solution.py:40
  144.1 1.3 copy-done.10
  145.4 5.4 %fusion.5 = f32[768,2048]{1,0:T(8,128)S(1)} fusion(bf16[2,2048,1024]{2,1,0:T(8,128)(2,1)} %all-gather.2.cloned.1.call-done, bf16[1,768,1024]{2,1,0:T(8,128)(2,1)S(1)} %copy-done.10), kind=kOutput, calls=%fused_computation.17 | convolution fusion | flops 3221225472 | bytes 12058624 | tf_op jit(solution)/shard_map/dot_general | solution.py:34
  150.9 7.3 %add_convert_fusion = bf16[768,2048]{1,0:T(8,128)(2,1)} fusion(f32[768,2048]{1,0:T(8,128)S(1)} %fusion.5, bf16[2,2048,1024]{2,1,0:T(8,128)(2,1)} %all-gather.2.cloned.1.call-done, f32[2,768,1024]{2,1,0:T(8,128)S(1)} %copy-done.3, bf16[768,1024]{1,0:T(8,128)(2,1)S(1)} %copy-done.8), kind=kOutput, calls=%fused_computation.7 | convolution fusion | flops 3226730496 | bytes 18350080 | tf_op jit(solution)/shard_map/dot_general | solution.py:34
  158.6 1.6 copy.18
  160.2 22.3 %all-reduce.6 = (f32[3,1024]{1,0:T(4,128)S(1)}, f32[1024]{0:T(1024)S(1)}) all-reduce(f32[3,1024]{1,0:T(4,128)S(1)} %pad_maximum_fusion.1, f32[1024]{0:T(1024)S(1)} %get-tuple-element.18), channel_id=1, replica_groups=mesh['fs'=8,'tp'=4] {'fs'}, use_global_device_ids=true, to_apply=%region_6.7 | all-reduce | flops 4096 | bytes 32768 | tf_op jit(solution)/shard_map/psum | solution.py:105
  183.1 0.6 multiply_add_fusion.2
  183.7 4.5 %fusion.23 = bf16[768,1024]{1,0:T(8,128)(2,1)} fusion(f32[2,768,1024]{2,1,0:T(8,128)} %bitcast.61, f32[2,768,1024]{2,1,0:T(8,128)} %copy-done.2), kind=kLoop, calls=%fused_computation.43 | loop fusion | flops 1572864 | bytes 7864320 | tf_op jit(solution)/shard_map/squeeze | solution.py:74
  188.2 1.3 multiply_add_fusion.1
  189.5 1.3 copy.19
  190.8 39.4 %reduce-scatter.5.cloned.1.call-done = bf16[256,1024]{0,1:T(8,128)(2,1)} async-done(((bf16[2048,1024]{0,1:T(8,128)(2,1)}), bf16[256,1024]{0,1:T(8,128)(2,1)}) %reduce-scatter.5.cloned.1.call-update) | async-done | bytes 524304 | tf_op jit(solution)/shard_map/reduce_scatter | solution.py:84
  230.2 1.2 multiply_add_fusion
  231.4 1.3 copy.20
  232.7 88.9 %all-reduce.9.cloned.1.call-done = bf16[768,2048]{1,0:T(8,128)(2,1)} async-done(((bf16[768,2048]{1,0:T(8,128)(2,1)}), bf16[768,2048]{1,0:T(8,128)(2,1)}) %all-reduce.9.cloned.1.call-update) | async-done | bytes 3145744 | tf_op jit(solution)/shard_map/psum | solution.py:94
  321.7 4.0 %copy.23 = bf16[768,2048]{1,0:T(8,128)(2,1)} copy(bf16[768,2048]{1,0:T(8,128)(2,1)} %all-reduce.9.cloned.1.call-done) | data formatting | bytes 6291456
  (41 shorter events, 2.0 us)
Async XLA Ops:
  7.2 3.5 %copy-start.4 = (bf16[768,2048]{1,0:T(8,128)(2,1)S(1)}, bf16[768,2048]{1,0:T(8,128)(2,1)}, u32[]{:S(2)}) copy-start(bf16[768,2048]{1,0:T(8,128)(2,1)} %param.11) | copy-start | bytes 9437188
  7.2 84.6 %all-gather.2.cloned.1.call-start = ((), (), s32[]{:S(2)}) async-start(), calls=%async_computation.2 | async-start | bytes 9437184 | tf_op jit(solution)/shard_map/all_gather | solution.py:62
  9.7 178.5 %reduce-scatter.3.cloned.1.call-start = ((), (), s32[]{:S(2)}) async-start(), calls=%async_computation.4 | async-start | bytes 4718592 | tf_op jit(solution)/shard_map/reduce_scatter | solution.py:89
  9.7 2.9 copy-start.5
  91.8 10.1 %copy-start.15 = (bf16[2,2048,1024]{2,1,0:T(8,128)(2,1)S(1)}, bf16[2,2048,1024]{2,1,0:T(8,128)(2,1)}, u32[]{:S(2)}) copy-start(bf16[2,2048,1024]{2,1,0:T(8,128)(2,1)} %all-gather.2.cloned.1.call-done) | copy-start | bytes 25165828
  113.4 0.7 copy-start.14
  114.1 3.8 %copy-start.1 = (f32[1536,1024]{1,0:T(8,128)}, f32[1536,1024]{1,0:T(8,128)S(1)}, u32[]{:S(2)}) copy-start(f32[1536,1024]{1,0:T(8,128)S(1)} %convert_element_type.60) | copy-start | bytes 18874372
  117.3 6.9 %copy-start = (f32[2,768,1024]{2,1,0:T(8,128)}, f32[2,768,1024]{2,1,0:T(8,128)S(1)}, u32[]{:S(2)}) copy-start(f32[2,768,1024]{2,1,0:T(8,128)S(1)} %get-tuple-element.24) | copy-start | bytes 18874372
  124.2 2.2 copy-start.6
  125.2 1.1 copy-start.9
  131.5 98.7 %reduce-scatter.5.cloned.1.call-start = ((), (), s32[]{:S(2)}) async-start(), calls=%async_computation.5 | async-start | bytes 4718592 | tf_op jit(solution)/shard_map/reduce_scatter | solution.py:84
  131.7 7.1 %copy-start.7 = (bf16[768,1024]{1,0:T(8,128)(2,1)S(1)}, bf16[768,1024]{1,0:T(8,128)(2,1)}, u32[]{:S(2)}) copy-start(bf16[768,1024]{1,0:T(8,128)(2,1)} %param.13) | copy-start | bytes 4718596
  136.3 2.6 copy-start.2
  144.0 1.4 copy-start.10
  144.0 6.8 %copy-start.8 = (bf16[768,1024]{1,0:T(8,128)(2,1)S(1)}, bf16[768,1024]{1,0:T(8,128)(2,1)}, u32[]{:S(2)}) copy-start(bf16[768,1024]{1,0:T(8,128)(2,1)} %param.13) | copy-start | bytes 4718596
  144.0 177.6 %all-reduce.9.cloned.1.call-start = ((), (), s32[]{:S(2)}) async-start(), calls=%async_computation.3 | async-start | bytes 6291456 | tf_op jit(solution)/shard_map/psum | solution.py:94
  145.4 5.5 %copy-start.3 = (f32[2,768,1024]{2,1,0:T(8,128)S(1)}, f32[2,768,1024]{2,1,0:T(8,128)}, u32[]{:S(2)}) copy-start(f32[2,768,1024]{2,1,0:T(8,128)} %copy-done.2) | copy-start | bytes 18874372
  150.9 7.4 %copy-start.11 = (f32[256,1024]{1,0:T(8,128)S(1)}, f32[256,1024]{1,0:T(8,128)}, u32[]{:S(2)}) copy-start(f32[256,1024]{1,0:T(8,128)} %param.18) | copy-start | bytes 3145732
  158.2 24.3 %copy-start.13 = (f32[1024]{0:T(1024)S(1)}, f32[1024]{0:T(1024)}, u32[]{:S(2)}) copy-start(f32[1024]{0:T(1024)} %param.21) | copy-start | bytes 12292
  158.2 24.9 %copy-start.12 = (f32[3,1024]{1,0:T(4,128)S(1)}, f32[3,1024]{1,0:T(4,128)}, u32[]{:S(2)}) copy-start(f32[3,1024]{1,0:T(4,128)} %param.20) | copy-start | bytes 36868
Sparse Core Ops, SparseCore 0:
  10.2 81.5 all-gather.1
  131.6 47.8 reduce-scatter.2
  181.8 48.3 reduce-scatter.4
  233.8 87.8 all-reduce.8
where the time goes:
time: 334 us; the launch traced here: 332 us
  waiting for transfers between devices  205 us (61%)
  matrix products  41.9 us (13%)
  other arithmetic  27.1 us (8%)
  blocking collectives  22.3 us (7%)
  local copies, waits for them, and re-layouts  21.1 us (6%)
  between operations  14 us (4%)
    psum x1, waiting for transfers between devices, on_device(): input_grad = lax.psum(partial_rows.astype(jnp.bfloat16), 'tp')  88.9 us
    all_gather x1, waiting for transfers between devices, on_device(): pieces = lax.all_gather(paired, 'fs', axis=1, tiled=True)  77 us
    reduce_scatter x1, waiting for transfers between devices, on_device(): lax.psum_scatter(make_term(up_grad).astype(jnp.bfloat16), 'fs', scatter_d...  39.4 us
    psum x1, blocking collectives, on_device(): tap_total, bias_total = lax.psum((tap_local, bias_local), 'fs')  22.3 us
    unnamed x38, local copies, waits for them, and re-layouts  16.1 us
    dot_general x2, matrix products, contract_last(): lax.dot_general(left, right, (((1,), (1,)), ((), ())), preferred_element_...  12.8 us
    dot_general x2, matrix products, contract_first(): lax.dot_general(left, right, (((0,), (0,)), ((), ())), preferred_element_...  10.2 us
    dot_general x1, matrix products, on_device(): jnp.dot(stacked_rows, pieces[1], preferred_element_type=jnp.float32)  10.1 us
  transfers between devices with their start and end apart: 4, of which 3 were waited for; matrix products, arithmetic and copies ran while one was open for 12% of the time, Pallas kernels for 0%

commit v1 on v0

--- a/solution.py
+++ b/solution.py
@@ -1,7 +1,369 @@
+import functools
+import math
+
 import jax
 import jax.numpy as jnp
 from jax import lax
+from jax.experimental import pallas as pl
+from jax.experimental.pallas import tpu as pltpu
 from jax.sharding import PartitionSpec as P
+
+MESH = pl.DeviceIdType.MESH
+VMEM_BYTES = 58 * 1024 * 1024
+
+
+def add_parts(target, parts, block):
+    width = target.shape[-1]
+    block = min(block, width)
+
+    def body(index, carry):
+        columns = pl.ds(pl.multiple_of(index * block, block), block)
+        total = parts[0][:, columns].astype(jnp.float32)
+        for part in parts[1:]:
+            total += part[:, columns].astype(jnp.float32)
+        target[:, columns] = total.astype(target.dtype)
+        return carry
+
+    lax.fori_loop(0, width // block, body, 0)
+
+
+def reduce_kernel(
+    chips,
+    side,
+    gate_ref,
+    up_ref,
+    rows_ref,
+    small_ref,
+    grads_out,
+    rows_out,
+    small_out,
+    ring,
+    pair,
+    first_in,
+    first_sum,
+    second_in,
+    rows_buf,
+    small_buf,
+    ring_send,
+    ring_recv,
+    pair_send,
+    pair_recv,
+    first_send,
+    first_recv,
+    second_send,
+    second_recv,
+    third_send,
+    third_recv,
+    fourth_send,
+    fourth_recv,
+    small_send,
+    small_recv,
+):
+    fs = lax.axis_index("fs")
+    tp = lax.axis_index("tp")
+    fs_size = 2 * chips
+    z = fs // 2
+    core = lax.rem(fs, 2)
+    partner = z * 2 + 1 - core
+    ty = tp // side
+    tx = lax.rem(tp, side)
+    firsts = (tx, ty)
+    seconds = (ty, tx)
+
+    def first_peer(half, k):
+        peer = lax.rem(firsts[half] + k, side)
+        return peer, (ty * side + peer if half == 0 else peer * side + tx)
+
+    def second_peer(half, k):
+        peer = lax.rem(seconds[half] + k, side)
+        return peer, (peer * side + tx if half == 0 else ty * side + peer)
+
+    barrier = pltpu.get_barrier_semaphore()
+    for k in range(1, fs_size):
+        pl.semaphore_signal(
+            barrier, inc=1, device_id={"fs": lax.rem(fs + k, fs_size)}, device_id_type=MESH
+        )
+    for half in range(2):
+        for k in range(1, side):
+            pl.semaphore_signal(
+                barrier, inc=1, device_id={"tp": first_peer(half, k)[1]}, device_id_type=MESH
+            )
+    pl.semaphore_wait(barrier, fs_size - 1 + 2 * (side - 1))
+
+    parts = (gate_ref, up_ref)
+
+    def pair_copy(d, half):
+        return pltpu.make_async_remote_copy(
+            src_ref=parts[half].at[2 * d + 1 - core],
+            dst_ref=pair.at[d, half],
+            send_sem=pair_send.at[d, half],
+            recv_sem=pair_recv.at[d, half],
+            device_id={"fs": partner},
+            device_id_type=MESH,
+        )
+
+    def ring_copy(way, d, half):
+        target = lax.rem(fs + (2 if way == 0 else fs_size - 2), fs_size)
+        return pltpu.make_async_remote_copy(
+            src_ref=ring.at[way, d, half],
+            dst_ref=ring.at[way, d, half],
+            send_sem=ring_send.at[way, d, half],
+            recv_sem=ring_recv.at[way, d, half],
+            device_id={"fs": target},
+            device_id_type=MESH,
+        )
+
+    def first_copy(half, k):
+        peer, device = first_peer(half, k)
+        return pltpu.make_async_remote_copy(
+            src_ref=rows_ref.at[half, peer],
+            dst_ref=first_in.at[half, k - 1],
+            send_sem=first_send.at[half, k - 1],
+            recv_sem=first_recv.at[half, k - 1],
+            device_id={"tp": device},
+            device_id_type=MESH,
+        )
+
+    def second_copy(half, k):
+        peer, device = second_peer(half, k)
+        return pltpu.make_async_remote_copy(
+            src_ref=first_sum.at[half, peer],
+            dst_ref=second_in.at[half, k - 1],
+            send_sem=second_send.at[half, k - 1],
+            recv_sem=second_recv.at[half, k - 1],
+            device_id={"tp": device},
+            device_id_type=MESH,
+        )
+
+    def third_copy(half, k, shown):
+        _, device = second_peer(half, k)
+        block = rows_buf.at[half, firsts[half], shown]
+        return pltpu.make_async_remote_copy(
+            src_ref=block,
+            dst_ref=block,
+            send_sem=third_send.at[half, k - 1],
+            recv_sem=third_recv.at[half, k - 1],
+            device_id={"tp": device},
+            device_id_type=MESH,
+        )
+
+    def fourth_copy(half, k, shown):
+        _, device = first_peer(half, k)
+        block = rows_buf.at[half, shown]
+        return pltpu.make_async_remote_copy(
+            src_ref=block,
+            dst_ref=block,
+            send_sem=fourth_send.at[half, k - 1],
+            recv_sem=fourth_recv.at[half, k - 1],
+            device_id={"tp": device},
+            device_id_type=MESH,
+        )
+
+    def small_copy(k, slot):
+        return pltpu.make_async_remote_copy(
+            src_ref=small_ref,
+            dst_ref=small_buf.at[slot],
+            send_sem=small_send.at[k - 1],
+            recv_sem=small_recv.at[k - 1],
+            device_id={"fs": lax.rem(fs + k, fs_size)},
+            device_id_type=MESH,
+        )
+
+    def start_first():
+        for k in range(1, side):
+            for half in range(2):
+                first_copy(half, k).start()
+
+    def start_second():
+        for half in range(2):
+            for k in range(1, side):
+                first_copy(half, k).wait_recv()
+            for j in range(side):
+                add_parts(
+                    first_sum.at[half, j],
+                    [rows_ref.at[half, firsts[half], j]]
+                    + [first_in.at[half, k, j] for k in range(side - 1)],
+                    256,
+                )
+            for k in range(1, side):
+                second_copy(half, k).start()
+
+    def start_third():
+        for half in range(2):
+            for k in range(1, side):
+                second_copy(half, k).wait_recv()
+            add_parts(
+                rows_buf.at[half, firsts[half], seconds[half]],
+                [first_sum.at[half, seconds[half]]]
+                + [second_in.at[half, k] for k in range(side - 1)],
+                256,
+            )
+            for k in range(1, side):
+                third_copy(half, k, seconds[half]).start()
+
+    def start_fourth():
+        for half in range(2):
+            for k in range(1, side):
+                third_copy(half, k, lax.rem(seconds[half] + side - k, side)).wait_recv()
+            for k in range(1, side):
+                fourth_copy(half, k, firsts[half]).start()
+
+    def finish_rows():
+        for half in range(2):
+            for k in range(1, side):
+                fourth_copy(half, k, lax.rem(firsts[half] + side - k, side)).wait_recv()
+        for half in range(2):
+            for i in range(side):
+                for j in range(side):
+                    add_parts(rows_out.at[half, i, j], [rows_buf.at[half, i, j]], 256)
+
+    def own(d, half):
+        return parts[half].at[2 * d + core]
+
+    def push(way, d, half, first_on_line):
+        pair_copy(d, half).wait_recv()
+        slot = ring.at[way, d, half]
+
+        @pl.when(first_on_line)
+        def _():
+            add_parts(slot, [own(d, half), pair.at[d, half]], 128)
+
+        @pl.when(jnp.logical_not(first_on_line))
+        def _():
+            ring_copy(way, d, half).wait_recv()
+            add_parts(slot, [own(d, half), pair.at[d, half], slot], 128)
+
+        ring_copy(way, d, half).start()
+
+    last = chips - 1
+
+    def ring_step(t, half):
+        if t < last:
+
+            @pl.when(t >= z)
+            def _():
+                push(0, last - t + z, half, z == 0)
+
+            @pl.when(t >= last - z)
+            def _():
+                push(1, t - last + z, half, z == last)
+
+            return
+        pair_copy(z, half).wait_recv()
+        target = grads_out.at[half]
+        base = [own(z, half), pair.at[z, half]]
+
+        @pl.when(z > 0)
+        def _():
+            ring_copy(0, z, half).wait_recv()
+
+        @pl.when(z < last)
+        def _():
+            ring_copy(1, z, half).wait_recv()
+
+        @pl.when(z == 0)
+        def _():
+            add_parts(target, base + [ring.at[1, z, half]], 128)
+
+        @pl.when(z == last)
+        def _():
+            add_parts(target, base + [ring.at[0, z, half]], 128)
+
+        @pl.when(jnp.logical_and(z > 0, z < last))
+        def _():
+            add_parts(target, base + [ring.at[0, z, half], ring.at[1, z, half]], 128)
+
+    start_first()
+    order = []
+    for s in range((chips + 1) // 2):
+        order += [last - s] + ([s] if s != last - s else [])
+    for d in order:
+        for half in range(2):
+            pair_copy(d, half).start()
+    small_buf[fs] = small_ref[...]
+    stages = {2: start_second, 3: start_third, 4: start_fourth, 5: finish_rows}
+    for t in range(chips):
+        for half in range(2):
+            ring_step(t, half)
+            if t == 0 and half == 1:
+                for k in range(1, fs_size):
+                    small_copy(k, fs).start()
+            if 2 * t + half in stages:
+                stages[2 * t + half]()
+
+    for k in range(1, fs_size):
+        small_copy(k, lax.rem(fs + fs_size - k, fs_size)).wait_recv()
+    total = small_buf[0]
+    for source in range(1, fs_size):
+        total += small_buf[source]
+    small_out[...] = total
+
+    for half in range(2):
+        for d in range(chips):
+            pair_copy(d, half).wait_send()
+        for k in range(1, side):
+            first_copy(half, k).wait_send()
+            second_copy(half, k).wait_send()
+            third_copy(half, k, seconds[half]).wait_send()
+            fourth_copy(half, k, firsts[half]).wait_send()
+        for d in range(chips):
+
+            @pl.when(z < d)
+            def _():
+                ring_copy(0, d, half).wait_send()
+
+            @pl.when(z > d)
+            def _():
+                ring_copy(1, d, half).wait_send()
+
+    for k in range(1, fs_size):
+        small_copy(k, fs).wait_send()
+
+
+def reduce_all(gate_part, up_part, partial_rows, small):
+    fs_size = lax.axis_size("fs")
+    chips = fs_size // 2
+    side = math.isqrt(lax.axis_size("tp"))
+    depth, width = gate_part.shape[0] // fs_size, gate_part.shape[1]
+    tokens, model = partial_rows.shape
+    r = tokens // (2 * side * side)
+    bf16, dma = jnp.bfloat16, pltpu.SemaphoreType.DMA
+    vmem = pl.BlockSpec(memory_space=pltpu.VMEM)
+    rows_shape = (2, side, side, r, model)
+    grads, rows, small_sum = pl.pallas_call(
+        functools.partial(reduce_kernel, chips, side),
+        out_shape=(
+            jax.ShapeDtypeStruct((2, depth, width), jnp.float32),
+            jax.ShapeDtypeStruct(rows_shape, bf16),
+            jax.ShapeDtypeStruct(small.shape, jnp.float32),
+        ),
+        in_specs=[vmem] * 4,
+        out_specs=(vmem, vmem, vmem),
+        scratch_shapes=[
+            pltpu.VMEM((2, chips, 2, depth, width), bf16),
+            pltpu.VMEM((chips, 2, depth, width), bf16),
+            pltpu.VMEM((2, side - 1, side, r, model), bf16),
+            pltpu.VMEM((2, side, r, model), bf16),
+            pltpu.VMEM((2, side - 1, r, model), bf16),
+            pltpu.VMEM(rows_shape, bf16),
+            pltpu.VMEM((fs_size,) + small.shape, jnp.float32),
+            dma((2, chips, 2)),
+            dma((2, chips, 2)),
+            dma((chips, 2)),
+            dma((chips, 2)),
+        ]
+        + [dma((2, side - 1))] * 8
+        + [dma((fs_size - 1,))] * 2,
+        compiler_params=pltpu.CompilerParams(
+            collective_id=0, has_side_effects=True, vmem_limit_bytes=VMEM_BYTES
+        ),
+    )(
+        gate_part.reshape(fs_size, depth, width),
+        up_part.reshape(fs_size, depth, width),
+        partial_rows.reshape(rows_shape),
+        small,
+    )
+    return grads[0], grads[1], rows.reshape(tokens, model), small_sum
 
 
 def shift_down(values, distance):
@@ -81,19 +443,11 @@
     mixed_back = mixed[1:]
     sig_back = sig_all[1:]
     up_grad = (cotangent * activated[1:]).astype(jnp.bfloat16)[0]
-    up_summed = lax.psum_scatter(
-        make_term(up_grad).astype(jnp.bfloat16), "fs", scatter_dimension=0, tiled=True
-    ).astype(jnp.float32)
+    up_part = make_term(up_grad).astype(jnp.bfloat16)
     mixed_grad = cotangent * up_float[1:] * sig_back * (1.0 + mixed_back * (1.0 - sig_back))
     gate_grad = mix_adjoint(mixed_grad, conv_taps).astype(jnp.bfloat16)[0]
-    gate_summed = lax.psum_scatter(
-        make_term(gate_grad).astype(jnp.bfloat16), "fs", scatter_dimension=0, tiled=True
-    ).astype(jnp.float32)
-    pieces = lax.all_gather(paired, "fs", axis=1, tiled=True)
+    gate_part = make_term(gate_grad).astype(jnp.bfloat16)
     partial_rows = contract_last(gate_grad, pieces[0]) + contract_last(up_grad, pieces[1])
-    input_grad = lax.psum(partial_rows.astype(jnp.bfloat16), "tp")
-    gate_grad_out = gate_grad_sum + grad_scale * gate_summed
-    up_grad_out = up_grad_sum + grad_scale * up_summed
     gate_back = gate_float[1:]
     tap_local = jnp.stack(
         [
@@ -102,7 +456,15 @@
         ]
     )
     bias_local = jnp.sum(mixed_grad, axis=(0, 1))
-    tap_total, bias_total = lax.psum((tap_local, bias_local), "fs")
+    taps = conv_taps.shape[0]
+    small = jnp.concatenate([tap_local, bias_local[None]], axis=0)
+    small = jnp.pad(small, ((0, -(taps + 1) % 8), (0, 0)))
+    gate_summed, up_summed, input_grad, small_sum = reduce_all(
+        gate_part, up_part, partial_rows.astype(jnp.bfloat16), small
+    )
+    tap_total, bias_total = small_sum[:taps], small_sum[taps]
+    gate_grad_out = gate_grad_sum + grad_scale * gate_summed
+    up_grad_out = up_grad_sum + grad_scale * up_summed
     taps_grad_out = taps_grad_sum + grad_scale * tap_total
     bias_grad_out = bias_grad_sum + grad_scale * bias_total
     return (hidden_later, input_grad, gate_grad_out, up_grad_out, taps_grad_out, bias_grad_out)

time: 334 us -> 271 us (0.81)
  waiting for transfers between devices: 205 us -> 77.1 us
  Pallas kernels: 0 us -> 87.9 us
  blocking collectives: 22.3 us -> 0 us
  other arithmetic: 27.1 us -> 22.9 us
    psum x1 -> x0, waiting for transfers between devices: 88.9 us -> none  [on_device(): input_grad = lax.psum(partial_rows.astype(jnp.bfloat16), 'tp')]
    pallas_call x0 -> x1, Pallas kernels: none -> 87.9 us  [reduce_all(): pl.pallas_call(functools.partial(reduce_kernel, chips, side), out_shape=(...]
    reduce_scatter x2 -> x0, waiting for transfers between devices: 39.4 us -> none  [the longest x1 39.4 us: on_device(): lax.psum_scatter(make_term(up_grad).astype(jnp.bfloat16), 'fs', scatter_d...]
    psum x1 -> x0, blocking collectives: 22.3 us -> none  [on_device(): tap_total, bias_total = lax.psum((tap_local, bias_local), 'fs')]
    convert_element_type x0 -> x2, local copies, waits for them, and re-layouts: none -> 13 us  [the longest x1 6.57 us: on_device(): up_part = make_term(up_grad).astype(jnp.bfloat16)]
    unnamed x38 -> x34, local copies, waits for them, and re-layouts: 16.1 us -> 5.7 us
  transfers between devices with their start and end apart: 4 -> 1, of which waited for: 3 -> 1; matrix products, arithmetic and copies ran while one was open for 12% -> 2% of each run, Pallas kernels for 0% -> 0%
where the time goes in v1:
time: 271 us
  Pallas kernels  87.9 us (32%)
  waiting for transfers between devices  77.1 us (28%)
  matrix products  44.8 us (17%)
  local copies, waits for them, and re-layouts  23.6 us (9%)
  other arithmetic  22.9 us (8%)
  between operations  14.2 us (5%)
    pallas_call x1, Pallas kernels, reduce_all(): pl.pallas_call(functools.partial(reduce_kernel, chips, side), out_shape=(...  87.9 us
    all_gather x1, waiting for transfers between devices, on_device(): pieces = lax.all_gather(paired, 'fs', axis=1, tiled=True)  77.1 us
    dot_general x2, matrix products, contract_last(): lax.dot_general(left, right, (((1,), (1,)), ((), ())), preferred_element_...  13 us
    dot_general x2, matrix products, contract_first(): lax.dot_general(left, right, (((0,), (0,)), ((), ())), preferred_element_...  12.9 us
    dot_general x1, matrix products, on_device(): jnp.dot(stacked_rows, pieces[1], preferred_element_type=jnp.float32)  10.1 us
    dot_general x1, matrix products, on_device(): jnp.dot(stacked_rows, pieces[0], preferred_element_type=jnp.float32)  8.82 us
    convert_element_type x1, local copies, waits for them, and re-layouts, on_device(): up_part = make_term(up_grad).astype(jnp.bfloat16)  6.57 us
    convert_element_type x1, local copies, waits for them, and re-layouts, on_device(): gate_part = make_term(gate_grad).astype(jnp.bfloat16)  6.41 us
  transfers between devices with their start and end apart: 1, of which 1 were waited for; matrix products, arithmetic and copies ran while one was open for 2% of the time, Pallas kernels for 0%

profile of v1, /device:TPU:16, one launch (start us, length us, event | category | flops | bytes accessed | tf_op | source)
XLA Modules:
  0.0 270.6 jit_solution(9985500607924230576)
XLA Ops:
  7.2 0.0 all-gather.2.cloned.1.call-start
  7.2 2.4 pad_maximum_fusion
  9.6 0.0 all-gather.2.cloned.1.call-update
  9.7 0.9 fusion.32
  10.6 1.9 constant_dynamic-update-slice_fusion.1
  12.6 2.1 constant_dynamic-update-slice_fusion
  14.7 77.1 %all-gather.2.cloned.1.call-done = bf16[2,2048,1024]{2,1,0:T(8,128)(2,1)} async-done(((bf16[2,256,1024]{2,1,0:T(8,128)(2,1)}), bf16[2,2048,1024]{2,1,0:T(8,128)(2,1)}) %all-gather.2.cloned.1.call-update) | async-done | bytes 8388624 | tf_op jit(solution)/shard_map/all_gather | solution.py:424
  91.8 10.1 %convolution_convert_fusion = bf16[1536,1024]{1,0:T(8,128)(2,1)S(1)} fusion(bf16[1536,2048]{1,0:T(8,128)(2,1)} %constant_dynamic-update-slice_fusion, bf16[2,2048,1024]{2,1,0:T(8,128)(2,1)} %all-gather.2.cloned.1.call-done), kind=kOutput, calls=%fused_computation.15 | convolution fusion | flops 6444023808 | bytes 13631488 | tf_op jit(solution)/shard_map/dot_general | solution.py:426
  102.0 8.8 %convolution_convert_fusion.1 = bf16[1536,1024]{1,0:T(8,128)(2,1)S(1)} fusion(bf16[1536,2048]{1,0:T(8,128)(2,1)} %constant_dynamic-update-slice_fusion, bf16[2,2048,1024]{2,1,0:T(8,128)(2,1)S(1)} %copy-done.13), kind=kOutput, calls=%fused_computation.16 | convolution fusion | flops 6444023808 | bytes 13631488 | tf_op jit(solution)/shard_map/dot_general | solution.py:425
  110.8 0.7 convert_element_type.55
  111.5 1.9 slice_bitcast_fusion.6
  113.4 0.7 convert_element_type.56
  114.1 3.2 %add_divide_fusion = (f32[2,768,1024]{2,1,0:T(8,128)S(1)}, f32[2,768,1024]{2,1,0:T(8,128)S(1)}) fusion(f32[1024]{0:T(1024)S(1)} %copy-done.12, f32[2,768,1024]{2,1,0:T(8,128)S(1)} %bitcast.70, f32[1024]{0:T(1024)S(1)} %bitcast.82, f32[1024]{0:T(1024)S(1)} %bitcast.84, f32[1024]{0:T(1024)S(1)} %bitcast.80), kind=kLoop, calls=%fused_computation.8 | loop fusion | flops 14155776 | bytes 18890752 | tf_op jit(solution)/shard_map/div | solution.py:433
  117.3 1.6 fusion.29
  119.0 1.6 fusion.23
  120.6 0.9 copy-done.5
  121.5 7.7 %convert_bitcast_fusion = bf16[2048,1024]{0,1:T(8,128)(2,1)} fusion(bf16[768,2048]{1,0:T(8,128)(2,1)} %param.12, f32[2,768,1024]{2,1,0:T(8,128)S(1)} %fusion.29, bf16[768,1024]{1,0:T(8,128)(2,1)S(1)} %copy-done.5), kind=kOutput, calls=%fused_computation.11 | convolution fusion | flops 3225681920 | bytes 12058624 | tf_op jit(solution)/shard_map/dot_general | solution.py:402
  129.2 4.6 %fusion.13 = (f32[1024]{0:T(1024)S(1)}, f32[1024]{0:T(1024)S(1)}, f32[1024]{0:T(1024)S(1)}, f32[1024]{0:T(1024)S(1)}, f32[1,768,1024]{2,1,0:T(8,128)S(1)}) fusion(f32[1,768,1024]{2,1,0:T(8,128)} %slice_bitcast_fusion.6, f32[1536,1024]{1,0:T(8,128)S(1)} %convert_element_type.55, f32[2,768,1024]{2,1,0:T(8,128)S(1)} %get-tuple-element.22, ...), kind=kLoop, calls=%fused_computation.29 | loop fusion | flops 11005952 | bytes 20463616 | tf_op jit(solution)/shard_map/reduce_sum | solution.py:454
  133.8 1.0 fusion.10
  134.9 1.1 copy-done.7
  136.0 5.1 %convert_bitcast_fusion.1 = bf16[2048,1024]{0,1:T(8,128)(2,1)} fusion(bf16[768,2048]{1,0:T(8,128)(2,1)S(1)} %copy-done.3, bf16[1,768,1024]{2,1,0:T(8,128)(2,1)S(1)} %fusion.10), kind=kOutput, calls=%fused_computation.12 | convolution fusion | flops 3223322624 | bytes 8912896 | tf_op jit(solution)/shard_map/dot_general | solution.py:402
  141.1 6.4 %copy.17 = bf16[2048,1024]{1,0:T(8,128)(2,1)} copy(bf16[2048,1024]{0,1:T(8,128)(2,1)} %convert_bitcast_fusion.1) | data formatting | bytes 8388608 | tf_op jit(solution)/shard_map/convert_element_type | solution.py:449
  147.5 6.6 %copy.18 = bf16[2048,1024]{1,0:T(8,128)(2,1)} copy(bf16[2048,1024]{0,1:T(8,128)(2,1)} %convert_bitcast_fusion) | data formatting | bytes 8388608 | tf_op jit(solution)/shard_map/convert_element_type | solution.py:446
  154.1 0.6 select_maximum_fusion.small_ref
  154.7 5.9 %fusion.5 = f32[768,2048]{1,0:T(8,128)S(1)} fusion(bf16[2,2048,1024]{2,1,0:T(8,128)(2,1)} %all-gather.2.cloned.1.call-done, bf16[1,768,1024]{2,1,0:T(8,128)(2,1)} %copy-done.7), kind=kOutput, calls=%fused_computation.17 | convolution fusion | flops 3221225472 | bytes 12058624 | tf_op jit(solution)/shard_map/dot_general | solution.py:396
  160.6 7.2 %add_convert_fusion = bf16[768,2048]{1,0:T(8,128)(2,1)} fusion(f32[768,2048]{1,0:T(8,128)S(1)} %fusion.5, bf16[2,2048,1024]{2,1,0:T(8,128)(2,1)} %all-gather.2.cloned.1.call-done, f32[2,768,1024]{2,1,0:T(8,128)S(1)} %bitcast.75, bf16[768,1024]{1,0:T(8,128)(2,1)S(1)} %copy-done.6), kind=kOutput, calls=%fused_computation.7 | convolution fusion | flops 3226730496 | bytes 18350080 | tf_op jit(solution)/shard_map/dot_general | solution.py:396
  167.8 87.9 %shard_map.154 = (f32[2,256,1024]{2,1,0:T(8,128)}, bf16[2,2,2,96,2048]{4,3,2,1,0:T(8,128)(2,1)}, f32[8,1024]{1,0:T(8,128)}) custom-call(bf16[8,256,1024]{2,1,0:T(8,128)(2,1)} %bitcast.72, bf16[8,256,1024]{2,1,0:T(8,128)(2,1)} %bitcast.73, bf16[2,2,2,96,2048]{4,3,2,1,0:T(8,128)(2,1)} %bitcast.77, f32[8,1024]{1,0:T(8,128)} %select_maximum_fusion.small_ref), custom_call_target="tpu_custom_call" | custom-call | tf_op jit(solution)/shard_map/pallas_call | solution.py:333
  255.7 0.9 slice_multiply_fusion.2
  256.7 1.4 multiply_add_fusion
  258.1 0.6 add.67
  258.7 3.5 %bitcast_add_fusion = (f32[256,1024]{1,0:T(8,128)}, f32[256,1024]{1,0:T(8,128)}) fusion(f32[256,1024]{1,0:T(8,128)S(1)} %copy-done.8, f32[2,256,1024]{2,1,0:T(8,128)} %get-tuple-element.14, f32[256,1024]{1,0:T(8,128)S(1)} %copy-done.9), kind=kLoop, calls=%fused_computation.48 | loop fusion | flops 1048576 | bytes 6291456 | tf_op jit(solution)/shard_map/add | solution.py:467
  262.1 1.7 copy.21
  (31 shorter events, 0.1 us)
Async XLA Ops:
  7.2 3.4 %copy-start.1 = (bf16[768,2048]{1,0:T(8,128)(2,1)S(1)}, bf16[768,2048]{1,0:T(8,128)(2,1)}, u32[]{:S(2)}) copy-start(bf16[768,2048]{1,0:T(8,128)(2,1)} %param.11) | copy-start | bytes 9437188
  7.2 84.6 %all-gather.2.cloned.1.call-start = ((), (), s32[]{:S(2)}) async-start(), calls=%async_computation | async-start | bytes 9437184 | tf_op jit(solution)/shard_map/all_gather | solution.py:424
  9.7 2.9 %copy-start.2 = (bf16[768,2048]{1,0:T(8,128)(2,1)S(1)}, bf16[768,2048]{1,0:T(8,128)(2,1)}, u32[]{:S(2)}) copy-start(bf16[768,2048]{1,0:T(8,128)(2,1)} %param.12) | copy-start | bytes 9437188
  91.8 10.1 %copy-start.13 = (bf16[2,2048,1024]{2,1,0:T(8,128)(2,1)S(1)}, bf16[2,2048,1024]{2,1,0:T(8,128)(2,1)}, u32[]{:S(2)}) copy-start(bf16[2,2048,1024]{2,1,0:T(8,128)(2,1)} %all-gather.2.cloned.1.call-done) | copy-start | bytes 25165828
  113.4 0.7 copy-start.12
  119.0 10.3 %copy-start = (f32[2,768,1024]{2,1,0:T(8,128)}, f32[2,768,1024]{2,1,0:T(8,128)S(1)}, u32[]{:S(2)}) copy-start(f32[2,768,1024]{2,1,0:T(8,128)S(1)} %fusion.29) | copy-start | bytes 18874372
  119.0 2.5 copy-start.5
  133.8 2.2 copy-start.3
  134.8 1.1 copy-start.7
  147.5 13.1 %slice-start = ((s8[6291456]{0:T(1024)(128)(4,1)}), s8[2097152]{0:T(1024)(128)(4,1)S(1)}, s32[]{:S(2)}) async-start(s8[6291456]{0:T(1024)(128)(4,1)} %bitcast.74), calls=%async_computation.1 | async-start | bytes 4194304
  154.7 5.9 %slice-start.1 = ((s8[6291456]{0:T(1024)(128)(4,1)}), s8[4194304]{0:T(1024)(128)(4,1)S(1)}, s32[]{:S(2)}) async-start(s8[6291456]{0:T(1024)(128)(4,1)} %bitcast.74), calls=%async_computation.2 | async-start | bytes 8388608
  154.7 5.9 %copy-start.6 = (bf16[768,1024]{1,0:T(8,128)(2,1)S(1)}, bf16[768,1024]{1,0:T(8,128)(2,1)}, u32[]{:S(2)}) copy-start(bf16[768,1024]{1,0:T(8,128)(2,1)} %param.13) | copy-start | bytes 4718596
  167.8 88.9 %copy-start.10 = (f32[3,1024]{1,0:T(4,128)S(1)}, f32[3,1024]{1,0:T(4,128)}, u32[]{:S(2)}) copy-start(f32[3,1024]{1,0:T(4,128)} %param.20) | copy-start | bytes 36868
  167.8 90.3 %copy-start.11 = (f32[1024]{0:T(1024)S(1)}, f32[1024]{0:T(1024)}, u32[]{:S(2)}) copy-start(f32[1024]{0:T(1024)} %param.21) | copy-start | bytes 12292
  167.8 90.9 %copy-start.8 = (f32[256,1024]{1,0:T(8,128)S(1)}, f32[256,1024]{1,0:T(8,128)}, u32[]{:S(2)}) copy-start(f32[256,1024]{1,0:T(8,128)} %param.19) | copy-start | bytes 3145732
  167.8 90.9 %copy-start.9 = (f32[256,1024]{1,0:T(8,128)S(1)}, f32[256,1024]{1,0:T(8,128)}, u32[]{:S(2)}) copy-start(f32[256,1024]{1,0:T(8,128)} %param.18) | copy-start | bytes 3145732
  255.7 6.4 %copy-start.4 = (bf16[2,2,2,96,2048]{4,3,2,1,0:T(8,128)(2,1)S(1)}, bf16[2,2,2,96,2048]{4,3,2,1,0:T(8,128)(2,1)}, u32[]{:S(2)}) copy-start(bf16[2,2,2,96,2048]{4,3,2,1,0:T(8,128)(2,1)} %get-tuple-element.13) | copy-start | bytes 9437188
Sparse Core Ops, SparseCore 0:
  10.2 81.5 all-gather.1

commit v2 on v1

--- a/solution.py
+++ b/solution.py
@@ -404,6 +404,188 @@
     )
 
 
+def gather_kernel(
+    chips,
+    later_ref,
+    earlier_ref,
+    gate_ref,
+    up_ref,
+    weights,
+    gate_out,
+    up_out,
+    acc,
+    own_sem,
+    line_send,
+    line_recv,
+    pair_send,
+    pair_recv,
+):
+    fs = lax.axis_index("fs")
+    fs_size = 2 * chips
+    z = fs // 2
+    core = lax.rem(fs, 2)
+    last = chips - 1
+    depth = gate_ref.shape[0]
+    tokens = later_ref.shape[0]
+    block = math.gcd(tokens, 256)
+    parts = (gate_ref, up_ref)
+    outs = (gate_out, up_out)
+    neighbours = (lax.rem(fs + 2, fs_size), lax.rem(fs + fs_size - 2, fs_size))
+    partner = 2 * z + 1 - core
+
+    barrier = pltpu.get_barrier_semaphore()
+    for device in neighbours + (partner,):
+        pl.semaphore_signal(barrier, inc=1, device_id={"fs": device}, device_id_type=MESH)
+    pl.semaphore_wait(barrier, 3)
+
+    def shard(d, half, which):
+        return weights.at[half, d, pl.ds(pl.multiple_of(which * depth, depth), depth)]
+
+    def own_copy(half):
+        return pltpu.make_async_copy(parts[half], shard(z, half, core), own_sem.at[half])
+
+    def line_copy(way, d, half, own):
+        return pltpu.make_async_remote_copy(
+            src_ref=parts[half] if own else shard(d, half, core),
+            dst_ref=shard(d, half, core),
+            send_sem=line_send.at[way, d, half],
+            recv_sem=line_recv.at[d, half],
+            device_id={"fs": neighbours[way]},
+            device_id_type=MESH,
+        )
+
+    def pair_copy(d, half, own, which):
+        return pltpu.make_async_remote_copy(
+            src_ref=parts[half] if own else shard(d, half, which),
+            dst_ref=shard(d, half, which),
+            send_sem=pair_send.at[d, half],
+            recv_sem=pair_recv.at[d, half],
+            device_id={"fs": partner},
+            device_id_type=MESH,
+        )
+
+    def multiply(d, half, first):
+        columns = pl.ds(pl.multiple_of(d * 2 * depth, 2 * depth), 2 * depth)
+        for micro, rows_ref in enumerate((later_ref, earlier_ref)):
+
+            def body(index, carry):
+                rows = pl.ds(pl.multiple_of(index * block, block), block)
+                value = jnp.dot(
+                    rows_ref[rows, columns],
+                    weights[half, d],
+                    preferred_element_type=jnp.float32,
+                )
+                if first:
+                    acc[half, micro, rows] = value
+                else:
+                    acc[half, micro, rows] += value
+                return carry
+
+            lax.fori_loop(0, tokens // block, body, 0)
+
+    for half in range(2):
+
+        @pl.when(z < last)
+        def _():
+            line_copy(0, z, half, True).start()
+
+        @pl.when(z > 0)
+        def _():
+            line_copy(1, z, half, True).start()
+
+        pair_copy(z, half, True, core).start()
+        own_copy(half).start()
+
+    for half in range(2):
+        own_copy(half).wait()
+        pair_copy(z, half, True, 1 - core).wait_recv()
+        multiply(z, half, True)
+
+    def arrive(way, d, half, goes_on):
+        line_copy(way, d, half, False).wait_recv()
+
+        @pl.when(goes_on)
+        def _():
+            line_copy(way, d, half, False).start()
+
+        pair_copy(d, half, False, core).start()
+
+    def use(d, half):
+        pair_copy(d, half, False, 1 - core).wait_recv()
+        multiply(d, half, False)
+
+    for s in range(1, chips):
+        for half in range(2):
+
+            @pl.when(z - s >= 0)
+            def _():
+                arrive(0, z - s, half, z < last)
+
+            @pl.when(z + s <= last)
+            def _():
+                arrive(1, z + s, half, z > 0)
+
+            @pl.when(z - s >= 0)
+            def _():
+                use(z - s, half)
+
+            @pl.when(z + s <= last)
+            def _():
+                use(z + s, half)
+
+    for half in range(2):
+        for micro in range(2):
+
+            def body(index, carry):
+                rows = pl.ds(pl.multiple_of(index * block, block), block)
+                outs[half][micro, rows] = acc[half, micro, rows].astype(outs[half].dtype)
+                return carry
+
+            lax.fori_loop(0, tokens // block, body, 0)
+
+    for half in range(2):
+        for d in range(chips):
+            pair_copy(d, half, False, core).wait_send()
+
+            @pl.when(jnp.logical_and(d <= z, z < last))
+            def _():
+                line_copy(0, d, half, False).wait_send()
+
+            @pl.when(jnp.logical_and(d >= z, z > 0))
+            def _():
+                line_copy(1, d, half, False).wait_send()
+
+
+def gather_multiply(rows_later, rows_earlier, gate_proj, up_proj):
+    chips = lax.axis_size("fs") // 2
+    tokens = rows_later.shape[0]
+    depth, width = gate_proj.shape
+    bf16, dma = jnp.bfloat16, pltpu.SemaphoreType.DMA
+    vmem = pl.BlockSpec(memory_space=pltpu.VMEM)
+    weights, gate_pre, up_value = pl.pallas_call(
+        functools.partial(gather_kernel, chips),
+        out_shape=(
+            jax.ShapeDtypeStruct((2, chips, 2 * depth, width), bf16),
+            jax.ShapeDtypeStruct((2, tokens, width), bf16),
+            jax.ShapeDtypeStruct((2, tokens, width), bf16),
+        ),
+        in_specs=[vmem] * 4,
+        out_specs=(vmem, vmem, vmem),
+        scratch_shapes=[
+            pltpu.VMEM((2, 2, tokens, width), jnp.float32),
+            dma((2,)),
+            dma((2, chips, 2)),
+            dma((chips, 2)),
+            dma((chips, 2)),
+            dma((chips, 2)),
+        ],
+        compiler_params=pltpu.CompilerParams(
+            collective_id=1, has_side_effects=True, vmem_limit_bytes=VMEM_BYTES
+        ),
+    )(rows_later, rows_earlier, gate_proj, up_proj)
+    return weights.reshape(2, -1, width), gate_pre, up_value
+
+
 def on_device(
     rows_later,
     rows_earlier,
@@ -418,17 +600,9 @@
     bias_grad_sum,
 ):
     seq_len = rows_later.shape[0]
-    shard_width = out_cotangent.shape[1]
-    stacked_rows = jnp.concatenate([rows_later, rows_earlier], axis=0)
-    paired = jnp.stack([gate_proj, up_proj], axis=0)
-    pieces = lax.all_gather(paired, "fs", axis=1, tiled=True)
-    gate_acc = jnp.dot(stacked_rows, pieces[0], preferred_element_type=jnp.float32)
-    up_acc = jnp.dot(stacked_rows, pieces[1], preferred_element_type=jnp.float32)
-    gate_pre = gate_acc.astype(jnp.bfloat16)
-    up_value = up_acc.astype(jnp.bfloat16)
-    gate_pre, up_value = lax.optimization_barrier((gate_pre, up_value))
-    gate_float = gate_pre.astype(jnp.float32).reshape(2, seq_len, shard_width)
-    up_float = up_value.astype(jnp.float32).reshape(2, seq_len, shard_width)
+    pieces, gate_pre, up_value = gather_multiply(rows_later, rows_earlier, gate_proj, up_proj)
+    gate_float = gate_pre.astype(jnp.float32)
+    up_float = up_value.astype(jnp.float32)
     mixed = causal_mix(gate_float, conv_taps, conv_bias)
     sig_all = jax.nn.sigmoid(mixed)
     activated = mixed * sig_all

time: 271 us -> 247 us (0.911)
  Pallas kernels: 87.9 us -> 171 us
  waiting for transfers between devices: 77.1 us -> 0 us
  matrix products: 44.8 us -> 20.5 us
  between operations: 14.2 us -> 0.76 us
  other arithmetic: 22.9 us -> 29.9 us
    pallas_call x0 -> x1, Pallas kernels: none -> 77.6 us  [gather_multiply(): pl.pallas_call(functools.partial(gather_kernel, chips), out_shape=(jax.Sh...]
    all_gather x1 -> x0, waiting for transfers between devices: 77.1 us -> none  [on_device(): pieces = lax.all_gather(paired, 'fs', axis=1, tiled=True)]
    dot_general x2 -> x0, matrix products: 19 us -> none  [the longest x1 10.1 us: on_device(): jnp.dot(stacked_rows, pieces[1], preferred_element_type=jnp.float32)]
    pallas_call x1, Pallas kernels: 87.9 us -> 93.4 us  [reduce_all(): pl.pallas_call(functools.partial(reduce_kernel, chips, side), out_shape=(...]
    convert_element_type x1, other arithmetic: 0.99 us -> 5.32 us  [on_device(): gate_grad = mix_adjoint(mixed_grad, conv_taps).astype(jnp.bfloat16)[0]]
    dot_general x2, matrix products: 13 us -> 8.7 us  [contract_last(): lax.dot_general(left, right, (((1,), (1,)), ((), ())), preferred_element_...]
    slice x0 -> x1, local copies, waits for them, and re-layouts: none -> 3.69 us  [on_device(): pieces[1]]
    reduce_sum x1, other arithmetic: 4.58 us -> 7.52 us  [on_device(): jnp.sum(mixed_grad * shift_down(gate_back, 2 - tap_index), axis=(0, 1))]
  transfers between devices with their start and end apart: 1 -> 0, of which waited for: 1 -> 0; matrix products, arithmetic and copies ran while one was open for 2% -> 0% of each run, Pallas kernels for 0% -> 0%
where the time goes in v2:
time: 247 us
  Pallas kernels  171 us (69%)
  other arithmetic  29.9 us (12%)
  local copies, waits for them, and re-layouts  24.5 us (10%)
  matrix products  20.5 us (8%)
    pallas_call x1, Pallas kernels, reduce_all(): pl.pallas_call(functools.partial(reduce_kernel, chips, side), out_shape=(...  93.4 us
    pallas_call x1, Pallas kernels, gather_multiply(): pl.pallas_call(functools.partial(gather_kernel, chips), out_shape=(jax.Sh...  77.6 us
    dot_general x2, matrix products, contract_first(): lax.dot_general(left, right, (((0,), (0,)), ((), ())), preferred_element_...  11.8 us
    dot_general x2, matrix products, contract_last(): lax.dot_general(left, right, (((1,), (1,)), ((), ())), preferred_element_...  8.7 us
    reduce_sum x1, other arithmetic, on_device(): jnp.sum(mixed_grad * shift_down(gate_back, 2 - tap_index), axis=(0, 1))  7.52 us
    convert_element_type x1, local copies, waits for them, and re-layouts, on_device(): up_part = make_term(up_grad).astype(jnp.bfloat16)  6.55 us
    convert_element_type x1, local copies, waits for them, and re-layouts, on_device(): gate_part = make_term(gate_grad).astype(jnp.bfloat16)  6.41 us
    convert_element_type x1, other arithmetic, on_device(): gate_grad = mix_adjoint(mixed_grad, conv_taps).astype(jnp.bfloat16)[0]  5.32 us

profile of v2, /device:TPU:16, one launch (start us, length us, event | category | flops | bytes accessed | tf_op | source)
XLA Modules:
  0.0 246.6 jit_solution(5583803492991088367)
XLA Ops:
  0.6 0.8 fusion.30
  1.5 77.6 %shard_map.154 = (bf16[2,4,512,1024]{3,2,1,0:T(8,128)(2,1)}, bf16[2,768,1024]{2,1,0:T(8,128)(2,1)}, bf16[2,768,1024]{2,1,0:T(8,128)(2,1)}) custom-call(bf16[768,2048]{1,0:T(8,128)(2,1)} %later_ref.1, bf16[768,2048]{1,0:T(8,128)(2,1)} %earlier_ref.1, bf16[256,1024]{1,0:T(8,128)(2,1)} %gate_ref.1, bf16[256,1024]{1,0:T(8,128)(2,1)} %up_ref.1), custom_call_target="tpu_custom_call" | custom-call | tf_op jit(solution)/shard_map/pallas_call | solution.py:565
  79.1 0.0 copy-start
  79.1 2.8 %convert_element_type.46 = f32[2,768,1024]{2,1,0:T(8,128)S(1)} convert(bf16[2,768,1024]{2,1,0:T(8,128)(2,1)} %get-tuple-element.13) | non-fusion elementwise | flops 1572864 | bytes 9437184 | tf_op jit(solution)/shard_map/convert_element_type | solution.py:605
  81.9 0.0 copy-done
  81.9 2.1 slice.95
  84.0 0.7 convert_element_type.45
  84.7 0.5 slice-done
  85.2 1.5 slice-done.1
  86.7 3.7 %fusion.29 = (bf16[1,4,512,1024]{3,2,1,0:T(8,128)(2,1)}, bf16[1,4,512,1024]{3,2,1,0:T(8,128)(2,1)}) fusion(bf16[2,4,512,1024]{3,2,1,0:T(8,128)(2,1)S(1)} %bitcast.47), kind=kLoop, calls=%fused_computation.48 | loop fusion | bytes 16777216 | tf_op jit(solution)/shard_map/slice | solution.py:624
  90.4 0.0 copy-done.12
  90.4 4.7 %add_divide_fusion = (f32[2,768,1024]{2,1,0:T(8,128)}, f32[2,768,1024]{2,1,0:T(8,128)S(1)}) fusion(f32[1024]{0:T(1024)S(1)} %copy-done.12, f32[2,768,1024]{2,1,0:T(8,128)S(1)} %convert_element_type.45, f32[1024]{0:T(1024)S(1)} %bitcast.54, f32[1024]{0:T(1024)S(1)} %bitcast.56, f32[1024]{0:T(1024)S(1)} %bitcast.52), kind=kLoop, calls=%fused_computation.8 | loop fusion | flops 14155776 | bytes 18890752 | tf_op jit(solution)/shard_map/div | solution.py:607
  95.1 1.9 fusion.26
  97.0 7.5 %fusion.11 = (f32[1024]{0:T(1024)S(1)}, f32[1024]{0:T(1024)S(1)}, f32[1024]{0:T(1024)S(1)}, f32[1024]{0:T(1024)S(1)}, f32[1,768,1024]{2,1,0:T(8,128)}, /*index=5*/bf16[768,1024]{1,0:T(8,128)(2,1)}) fusion(f32[1,768,1024]{2,1,0:T(8,128)} %slice.95, f32[2,768,1024]{2,1,0:T(8,128)S(1)} %convert_element_type.45, f32[2,768,1024]{2,1,0:T(8,128)S(1)} %get-tuple-element.24, ...), kind=kLoop, calls=%fused_computation.23 | loop fusion | flops 12578816 | bytes 28327936 | tf_op jit(solution)/shard_map/reduce_sum | solution.py:628
  104.5 0.6 select_maximum_fusion.small_ref
  105.1 5.3 %fusion.8 = bf16[1,768,1024]{2,1,0:T(8,128)(2,1)S(1)} fusion(f32[1,768,1024]{2,1,0:T(8,128)} %get-tuple-element.22, f32[1024]{0:T(1024)S(1)} %bitcast.53, f32[1024]{0:T(1024)S(1)} %bitcast.57, f32[1024]{0:T(1024)S(1)} %bitcast.55), kind=kLoop, calls=%fused_computation.20 | loop fusion | flops 4718592 | bytes 4730880 | tf_op jit(solution)/shard_map/convert_element_type | solution.py:622
  110.5 0.0 copy-start.7
  110.5 1.2 copy-done.7
  111.6 3.5 %fusion.21 = f32[768,2048]{1,0:T(8,128)S(1)} fusion(bf16[2048,1024]{1,0:T(8,128)(2,1)S(1)} %bitcast.49, bf16[1,768,1024]{2,1,0:T(8,128)(2,1)S(1)} %fusion.8), kind=kOutput, calls=%fused_computation.36 | convolution fusion | flops 3221225472 | bytes 12058624 | tf_op jit(solution)/shard_map/dot_general | solution.py:396
  115.2 0.0 copy-start.3
  115.2 5.2 %add_convert_fusion = bf16[768,2048]{1,0:T(8,128)(2,1)} fusion(f32[768,2048]{1,0:T(8,128)S(1)} %fusion.21, bf16[2048,1024]{1,0:T(8,128)(2,1)S(1)} %bitcast.48, f32[2,768,1024]{2,1,0:T(8,128)S(1)} %fusion.26, bf16[768,1024]{1,0:T(8,128)(2,1)S(1)} %copy-done.6), kind=kOutput, calls=%fused_computation.7 | convolution fusion | flops 3226730496 | bytes 18350080 | tf_op jit(solution)/shard_map/dot_general | solution.py:396
  120.4 5.3 %convert_bitcast_fusion = bf16[2048,1024]{0,1:T(8,128)(2,1)} fusion(bf16[768,2048]{1,0:T(8,128)(2,1)S(1)} %copy-done.3, f32[2,768,1024]{2,1,0:T(8,128)S(1)} %fusion.26, bf16[768,1024]{1,0:T(8,128)(2,1)S(1)} %copy-done.6), kind=kOutput, calls=%fused_computation.9 | convolution fusion | flops 3225681920 | bytes 12058624 | tf_op jit(solution)/shard_map/dot_general | solution.py:402
  125.7 6.5 %copy.18 = bf16[2048,1024]{1,0:T(8,128)(2,1)} copy(bf16[2048,1024]{0,1:T(8,128)(2,1)} %convert_bitcast_fusion) | data formatting | bytes 8388608 | tf_op jit(solution)/shard_map/convert_element_type | solution.py:620
  132.2 0.0 copy-done.4
  132.2 6.5 %convert_bitcast_fusion.1 = bf16[2048,1024]{0,1:T(8,128)(2,1)} fusion(bf16[768,2048]{1,0:T(8,128)(2,1)S(1)} %copy-done.4, bf16[1,768,1024]{2,1,0:T(8,128)(2,1)} %copy-done.7), kind=kOutput, calls=%fused_computation.10 | convolution fusion | flops 3223322624 | bytes 8912896 | tf_op jit(solution)/shard_map/dot_general | solution.py:402
  138.7 6.4 %copy.17 = bf16[2048,1024]{1,0:T(8,128)(2,1)} copy(bf16[2048,1024]{0,1:T(8,128)(2,1)} %convert_bitcast_fusion.1) | data formatting | bytes 8388608 | tf_op jit(solution)/shard_map/convert_element_type | solution.py:623
  145.1 93.4 %shard_map.155 = (f32[2,256,1024]{2,1,0:T(8,128)}, bf16[2,2,2,96,2048]{4,3,2,1,0:T(8,128)(2,1)}, f32[8,1024]{1,0:T(8,128)}) custom-call(bf16[8,256,1024]{2,1,0:T(8,128)(2,1)} %bitcast.45, bf16[8,256,1024]{2,1,0:T(8,128)(2,1)} %bitcast.44, bf16[2,2,2,96,2048]{4,3,2,1,0:T(8,128)(2,1)} %bitcast.51, f32[8,1024]{1,0:T(8,128)} %select_maximum_fusion.small_ref), custom_call_target="tpu_custom_call" | custom-call | tf_op jit(solution)/shard_map/pallas_call | solution.py:333
  238.6 0.8 slice_multiply_fusion.2
  239.3 1.4 multiply_add_fusion
  240.7 0.6 add.67
  241.3 3.6 %bitcast_add_fusion = (f32[256,1024]{1,0:T(8,128)}, f32[256,1024]{1,0:T(8,128)}) fusion(f32[256,1024]{1,0:T(8,128)S(1)} %copy-done.8, f32[2,256,1024]{2,1,0:T(8,128)} %get-tuple-element.16, f32[256,1024]{1,0:T(8,128)S(1)} %copy-done.9), kind=kLoop, calls=%fused_computation.39 | loop fusion | flops 1048576 | bytes 6291456 | tf_op jit(solution)/shard_map/add | solution.py:641
  244.9 1.7 copy.20
  (22 shorter events, 0.0 us)
Async XLA Ops:
  79.1 2.8 %copy-start = (bf16[2,768,1024]{2,1,0:T(8,128)(2,1)S(1)}, bf16[2,768,1024]{2,1,0:T(8,128)(2,1)}, u32[]{:S(2)}) copy-start(bf16[2,768,1024]{2,1,0:T(8,128)(2,1)} %get-tuple-element.12) | copy-start | bytes 9437188
  81.9 3.3 %slice-start = ((s8[8388608]{0:T(1024)(128)(4,1)}), s8[4194304]{0:T(1024)(128)(4,1)S(1)}, s32[]{:S(2)}) async-start(s8[8388608]{0:T(1024)(128)(4,1)} %bitcast.46), calls=%async_computation | async-start | bytes 8388608
  84.0 2.8 %slice-start.1 = ((s8[8388608]{0:T(1024)(128)(4,1)}), s8[4194304]{0:T(1024)(128)(4,1)S(1)}, s32[]{:S(2)}) async-start(s8[8388608]{0:T(1024)(128)(4,1)} %bitcast.46), calls=%async_computation.1 | async-start | bytes 8388608
  86.7 3.7 %copy-start.12 = (f32[1024]{0:T(1024)S(1)}, f32[1024]{0:T(1024)}, u32[]{:S(2)}) copy-start(f32[1024]{0:T(1024)} %param.17) | copy-start | bytes 12292
  104.5 7.2 %copy-start.2 = (bf16[1,4,512,1024]{3,2,1,0:T(8,128)(2,1)S(1)}, bf16[1,4,512,1024]{3,2,1,0:T(8,128)(2,1)}, u32[]{:S(2)}) copy-start(bf16[1,4,512,1024]{3,2,1,0:T(8,128)(2,1)} %get-tuple-element.26) | copy-start | bytes 12582916
  110.5 1.2 copy-start.7
  111.6 3.5 %copy-start.1 = (bf16[1,4,512,1024]{3,2,1,0:T(8,128)(2,1)S(1)}, bf16[1,4,512,1024]{3,2,1,0:T(8,128)(2,1)}, u32[]{:S(2)}) copy-start(bf16[1,4,512,1024]{3,2,1,0:T(8,128)(2,1)} %get-tuple-element.25) | copy-start | bytes 12582916
  111.6 3.5 %copy-start.6 = (bf16[768,1024]{1,0:T(8,128)(2,1)S(1)}, bf16[768,1024]{1,0:T(8,128)(2,1)}, u32[]{:S(2)}) copy-start(bf16[768,1024]{1,0:T(8,128)(2,1)} %param.13) | copy-start | bytes 4718596
  115.2 5.2 %copy-start.3 = (bf16[768,2048]{1,0:T(8,128)(2,1)S(1)}, bf16[768,2048]{1,0:T(8,128)(2,1)}, u32[]{:S(2)}) copy-start(bf16[768,2048]{1,0:T(8,128)(2,1)} %earlier_ref.1) | copy-start | bytes 9437188
  125.7 6.6 %copy-start.4 = (bf16[768,2048]{1,0:T(8,128)(2,1)S(1)}, bf16[768,2048]{1,0:T(8,128)(2,1)}, u32[]{:S(2)}) copy-start(bf16[768,2048]{1,0:T(8,128)(2,1)} %earlier_ref.1) | copy-start | bytes 9437188
  145.1 94.2 %copy-start.10 = (f32[3,1024]{1,0:T(4,128)S(1)}, f32[3,1024]{1,0:T(4,128)}, u32[]{:S(2)}) copy-start(f32[3,1024]{1,0:T(4,128)} %param.20) | copy-start | bytes 36868
  145.1 95.6 %copy-start.11 = (f32[1024]{0:T(1024)S(1)}, f32[1024]{0:T(1024)}, u32[]{:S(2)}) copy-start(f32[1024]{0:T(1024)} %param.21) | copy-start | bytes 12292
  145.1 96.2 %copy-start.8 = (f32[256,1024]{1,0:T(8,128)S(1)}, f32[256,1024]{1,0:T(8,128)}, u32[]{:S(2)}) copy-start(f32[256,1024]{1,0:T(8,128)} %param.19) | copy-start | bytes 3145732
  145.1 96.2 %copy-start.9 = (f32[256,1024]{1,0:T(8,128)S(1)}, f32[256,1024]{1,0:T(8,128)}, u32[]{:S(2)}) copy-start(f32[256,1024]{1,0:T(8,128)} %param.18) | copy-start | bytes 3145732
  241.3 3.6 %copy-start.5 = (bf16[2,2,2,96,2048]{4,3,2,1,0:T(8,128)(2,1)S(1)}, bf16[2,2,2,96,2048]{4,3,2,1,0:T(8,128)(2,1)}, u32[]{:S(2)}) copy-start(bf16[2,2,2,96,2048]{4,3,2,1,0:T(8,128)(2,1)} %get-tuple-element.15) | copy-start | bytes 9437188

commit v3 on v2

--- a/solution.py
+++ b/solution.py
@@ -30,13 +30,17 @@
 def reduce_kernel(
     chips,
     side,
-    gate_ref,
-    up_ref,
-    rows_ref,
+    earlier_ref,
+    gate_grad_ref,
+    up_grad_ref,
+    weights_ref,
     small_ref,
-    grads_out,
+    gate_out,
+    up_out,
     rows_out,
     small_out,
+    terms,
+    rows_ref,
     ring,
     pair,
     first_in,
@@ -90,7 +94,38 @@
             )
     pl.semaphore_wait(barrier, fs_size - 1 + 2 * (side - 1))
 
-    parts = (gate_ref, up_ref)
+    parts = (terms.at[0], terms.at[1])
+    grad_refs = (gate_grad_ref, up_grad_ref)
+    outs = (gate_out, up_out)
+    depth = terms.shape[2]
+    wide = depth if depth % 128 == 0 else 2 * depth
+
+    def make_terms(d, half):
+        for piece in range(2 * depth // wide):
+            start = pl.multiple_of(d * 2 * depth + piece * wide, wide)
+            value = contract_first(earlier_ref[:, pl.ds(start, wide)], grad_refs[half][...])
+            for index in range(wide // depth):
+                rows = value[index * depth : (index + 1) * depth]
+                terms[half, 2 * d + piece + index] = rows.astype(terms.dtype)
+
+    def make_rows():
+        model = weights_ref.shape[1]
+        step = min(256, model)
+        r = rows_ref.shape[3]
+
+        def body(index, carry):
+            columns = pl.ds(pl.multiple_of(index * step, step), step)
+            value = contract_last(gate_grad_ref[...], weights_ref[0, columns])
+            value += contract_last(up_grad_ref[...], weights_ref[1, columns])
+            value = value.astype(rows_ref.dtype)
+            for half in range(2):
+                for i in range(side):
+                    for j in range(side):
+                        at = ((half * side + i) * side + j) * r
+                        rows_ref[half, i, j, :, columns] = value[at : at + r]
+            return carry
+
+        lax.fori_loop(0, model // step, body, 0)
 
     def pair_copy(d, half):
         return pltpu.make_async_remote_copy(
@@ -250,7 +285,7 @@
 
             return
         pair_copy(z, half).wait_recv()
-        target = grads_out.at[half]
+        target = outs[half]
         base = [own(z, half), pair.at[z, half]]
 
         @pl.when(z > 0)
@@ -273,21 +308,27 @@
         def _():
             add_parts(target, base + [ring.at[0, z, half], ring.at[1, z, half]], 128)
 
+    def in_turn(k):
+        return jnp.where(z < chips // 2, last - k, k)
+
+    for half in range(2):
+        make_terms(in_turn(0), half)
+        pair_copy(in_turn(0), half).start()
+    small_buf[fs] = small_ref[...]
+    for half in range(2):
+        ring_step(0, half)
+    make_rows()
     start_first()
-    order = []
-    for s in range((chips + 1) // 2):
-        order += [last - s] + ([s] if s != last - s else [])
-    for d in order:
+    for k in range(1, chips):
         for half in range(2):
-            pair_copy(d, half).start()
-    small_buf[fs] = small_ref[...]
-    stages = {2: start_second, 3: start_third, 4: start_fourth, 5: finish_rows}
-    for t in range(chips):
+            make_terms(in_turn(k), half)
+            pair_copy(in_turn(k), half).start()
+    for k in range(1, fs_size):
+        small_copy(k, fs).start()
+    stages = {3: start_second, 4: start_third, 5: start_fourth, 6: finish_rows}
+    for t in range(1, chips):
         for half in range(2):
             ring_step(t, half)
-            if t == 0 and half == 1:
-                for k in range(1, fs_size):
-                    small_copy(k, fs).start()
             if 2 * t + half in stages:
                 stages[2 * t + half]()
 
@@ -320,26 +361,29 @@
         small_copy(k, fs).wait_send()
 
 
-def reduce_all(gate_part, up_part, partial_rows, small):
+def reduce_all(rows_earlier, gate_grad, up_grad, weights, small):
     fs_size = lax.axis_size("fs")
     chips = fs_size // 2
     side = math.isqrt(lax.axis_size("tp"))
-    depth, width = gate_part.shape[0] // fs_size, gate_part.shape[1]
-    tokens, model = partial_rows.shape
+    tokens, model = rows_earlier.shape
+    depth, width = model // fs_size, gate_grad.shape[1]
     r = tokens // (2 * side * side)
     bf16, dma = jnp.bfloat16, pltpu.SemaphoreType.DMA
     vmem = pl.BlockSpec(memory_space=pltpu.VMEM)
     rows_shape = (2, side, side, r, model)
-    grads, rows, small_sum = pl.pallas_call(
+    gate_sum, up_sum, rows, small_sum = pl.pallas_call(
         functools.partial(reduce_kernel, chips, side),
         out_shape=(
-            jax.ShapeDtypeStruct((2, depth, width), jnp.float32),
+            jax.ShapeDtypeStruct((depth, width), jnp.float32),
+            jax.ShapeDtypeStruct((depth, width), jnp.float32),
             jax.ShapeDtypeStruct(rows_shape, bf16),
             jax.ShapeDtypeStruct(small.shape, jnp.float32),
         ),
-        in_specs=[vmem] * 4,
-        out_specs=(vmem, vmem, vmem),
+        in_specs=[vmem] * 5,
+        out_specs=(vmem, vmem, vmem, vmem),
         scratch_shapes=[
+            pltpu.VMEM((2, fs_size, depth, width), bf16),
+            pltpu.VMEM(rows_shape, bf16),
             pltpu.VMEM((2, chips, 2, depth, width), bf16),
             pltpu.VMEM((chips, 2, depth, width), bf16),
             pltpu.VMEM((2, side - 1, side, r, model), bf16),
@@ -357,13 +401,8 @@
         compiler_params=pltpu.CompilerParams(
             collective_id=0, has_side_effects=True, vmem_limit_bytes=VMEM_BYTES
         ),
-    )(
-        gate_part.reshape(fs_size, depth, width),
-        up_part.reshape(fs_size, depth, width),
-        partial_rows.reshape(rows_shape),
-        small,
-    )
-    return grads[0], grads[1], rows.reshape(tokens, model), small_sum
+    )(rows_earlier, gate_grad, up_grad, weights, small)
+    return gate_sum, up_sum, rows.reshape(tokens, model), small_sum
 
 
 def shift_down(values, distance):
@@ -610,18 +649,12 @@
     hidden_later = hidden[0]
     grad_scale = lax.rsqrt(jnp.asarray(seq_len * lax.axis_size("fs"), jnp.float32))
 
-    def make_term(grad_rows):
-        return contract_first(rows_earlier, grad_rows)
-
     cotangent = out_cotangent.astype(jnp.float32)[None]
     mixed_back = mixed[1:]
     sig_back = sig_all[1:]
     up_grad = (cotangent * activated[1:]).astype(jnp.bfloat16)[0]
-    up_part = make_term(up_grad).astype(jnp.bfloat16)
     mixed_grad = cotangent * up_float[1:] * sig_back * (1.0 + mixed_back * (1.0 - sig_back))
     gate_grad = mix_adjoint(mixed_grad, conv_taps).astype(jnp.bfloat16)[0]
-    gate_part = make_term(gate_grad).astype(jnp.bfloat16)
-    partial_rows = contract_last(gate_grad, pieces[0]) + contract_last(up_grad, pieces[1])
     gate_back = gate_float[1:]
     tap_local = jnp.stack(
         [
@@ -634,7 +667,7 @@
     small = jnp.concatenate([tap_local, bias_local[None]], axis=0)
     small = jnp.pad(small, ((0, -(taps + 1) % 8), (0, 0)))
     gate_summed, up_summed, input_grad, small_sum = reduce_all(
-        gate_part, up_part, partial_rows.astype(jnp.bfloat16), small
+        rows_earlier, gate_grad, up_grad, pieces, small
     )
     tap_total, bias_total = small_sum[:taps], small_sum[taps]
     gate_grad_out = gate_grad_sum + grad_scale * gate_summed

time: 247 us -> 213 us (0.86)
  matrix products: 20.5 us -> 0 us
  local copies, waits for them, and re-layouts: 24.5 us -> 4.66 us
  other arithmetic: 29.9 us -> 34.5 us
    dot_general x4 -> x0, matrix products: 20.5 us -> none  [the longest x2 11.8 us: contract_first(): lax.dot_general(left, right, (((0,), (0,)), ((), ())), preferred_element_...]
    squeeze x0 -> x2, other arithmetic: none -> 15.3 us  [the longest x1 9.1 us: on_device(): up_grad = (cotangent * activated[1:]).astype(jnp.bfloat16)[0]]
    convert_element_type x2 -> x0, local copies, waits for them, and re-layouts: 13 us -> none  [the longest x1 6.55 us: on_device(): up_part = make_term(up_grad).astype(jnp.bfloat16)]
    reduce_sum x1 -> x0, other arithmetic: 7.52 us -> none  [on_device(): jnp.sum(mixed_grad * shift_down(gate_back, 2 - tap_index), axis=(0, 1))]
    convert_element_type x1 -> x0, other arithmetic: 5.32 us -> none  [on_device(): gate_grad = mix_adjoint(mixed_grad, conv_taps).astype(jnp.bfloat16)[0]]
    slice x1 -> x0, local copies, waits for them, and re-layouts: 3.69 us -> none  [on_device(): pieces[1]]
    unnamed x31 -> x17, local copies, waits for them, and re-layouts: 4.94 us -> 1.75 us
where the time goes in v3:
time: 213 us; the launch traced here: 211 us
  Pallas kernels  171 us (80%)
  other arithmetic  34.5 us (16%)
  local copies, waits for them, and re-layouts  4.66 us (2%)
    pallas_call x1, Pallas kernels, reduce_all(): pl.pallas_call(functools.partial(reduce_kernel, chips, side), out_shape=(...  93.7 us
    pallas_call x1, Pallas kernels, gather_multiply(): pl.pallas_call(functools.partial(gather_kernel, chips), out_shape=(jax.Sh...  77.7 us
    squeeze x1, other arithmetic, on_device(): up_grad = (cotangent * activated[1:]).astype(jnp.bfloat16)[0]  9.1 us
    squeeze x1, other arithmetic, on_device(): gate_grad = mix_adjoint(mixed_grad, conv_taps).astype(jnp.bfloat16)[0]  6.15 us
    div x1, other arithmetic, on_device(): sig_all = jax.nn.sigmoid(mixed)  4.64 us

profile of v3, /device:TPU:16, one launch (start us, length us, event | category | flops | bytes accessed | tf_op | source)
XLA Modules:
  0.0 211.3 jit_solution(14174647794830113642)
XLA Ops:
  0.6 0.8 fusion.25
  1.5 77.7 %shard_map.154 = (bf16[2,4,512,1024]{3,2,1,0:T(8,128)(2,1)}, bf16[2,768,1024]{2,1,0:T(8,128)(2,1)}, bf16[2,768,1024]{2,1,0:T(8,128)(2,1)}) custom-call(bf16[768,2048]{1,0:T(8,128)(2,1)} %later_ref.1, bf16[768,2048]{1,0:T(8,128)(2,1)} %earlier_ref.3, bf16[256,1024]{1,0:T(8,128)(2,1)} %gate_ref.1, bf16[256,1024]{1,0:T(8,128)(2,1)} %up_ref.1), custom_call_target="tpu_custom_call" | custom-call | tf_op jit(solution)/shard_map/pallas_call | solution.py:604
  79.1 0.0 copy-start
  79.2 2.8 %convert_element_type.31 = f32[2,768,1024]{2,1,0:T(8,128)S(1)} convert(bf16[2,768,1024]{2,1,0:T(8,128)(2,1)} %get-tuple-element.14) | non-fusion elementwise | flops 1572864 | bytes 9437184 | tf_op jit(solution)/shard_map/convert_element_type | solution.py:644
  81.9 0.1 copy-done
  82.0 2.1 slice.77
  84.0 0.0 copy-start.7
  84.0 0.7 convert_element_type.30
  84.8 0.0 copy-done.7
  84.8 4.6 %add_divide_fusion = (f32[2,768,1024]{2,1,0:T(8,128)}, f32[2,768,1024]{2,1,0:T(8,128)S(1)}) fusion(f32[1024]{0:T(1024)S(1)} %copy-done.7, f32[2,768,1024]{2,1,0:T(8,128)S(1)} %convert_element_type.30, f32[1024]{0:T(1024)S(1)} %bitcast.25, f32[1024]{0:T(1024)S(1)} %bitcast.27, f32[1024]{0:T(1024)S(1)} %bitcast.23), kind=kLoop, calls=%fused_computation.7 | loop fusion | flops 14155776 | bytes 18890752 | tf_op jit(solution)/shard_map/div | solution.py:646
  89.4 0.0 copy-start.2
  89.4 4.2 %fusion.22 = f32[2,768,1024]{2,1,0:T(8,128)} fusion(f32[2,768,1024]{2,1,0:T(8,128)S(1)} %get-tuple-element.26), kind=kLoop, calls=%fused_computation.42 | loop fusion | flops 6291456 | bytes 12582912 | tf_op jit(solution)/shard_map/mul | solution.py:647
  93.6 0.0 copy-done.2
  93.6 9.1 %fusion.20 = (bf16[768,1024]{1,0:T(8,128)(2,1)}, bf16[768,1024]{1,0:T(8,128)(2,1)}, f32[1024]{0:T(1024)S(1)}, f32[1024]{0:T(1024)S(1)}, f32[1024]{0:T(1024)S(1)}, /*index=5*/f32[1024]{0:T(1024)S(1)}, f32[1,768,1024]{2,1,0:T(8,128)}) fusion(f32[2,768,1024]{2,1,0:T(8,128)} %fusion.22, bf16[768,1024]{1,0:T(8,128)(2,1)S(1)} %copy-done.2, ...), kind=kLoop, calls=%fused_computation.32 | loop fusion | flops 14151680 | bytes 33046528 | tf_op jit(solution)/shard_map/squeeze | solution.py:655
  102.7 0.6 select_maximum_fusion.small_ref
  103.3 6.2 %fusion.21.gate_grad_ref = bf16[768,1024]{1,0:T(8,128)(2,1)} fusion(f32[1,768,1024]{2,1,0:T(8,128)} %get-tuple-element.33, f32[1024]{0:T(1024)S(1)} %bitcast.24, f32[1024]{0:T(1024)S(1)} %bitcast.28, f32[1024]{0:T(1024)S(1)} %bitcast.26), kind=kLoop, calls=%fused_computation.33 | loop fusion | flops 4718592 | bytes 4730880 | tf_op jit(solution)/shard_map/squeeze | solution.py:657
  109.5 0.0 copy-start.5
  109.5 0.0 copy-start.6
  109.5 0.0 copy-start.3
  109.5 0.0 copy-start.4
  109.5 93.7 %shard_map.155 = (f32[256,1024]{1,0:T(8,128)}, f32[256,1024]{1,0:T(8,128)}, bf16[2,2,2,96,2048]{4,3,2,1,0:T(8,128)(2,1)}, f32[8,1024]{1,0:T(8,128)}) custom-call(bf16[768,2048]{1,0:T(8,128)(2,1)} %earlier_ref.3, bf16[768,1024]{1,0:T(8,128)(2,1)} %fusion.21.gate_grad_ref, bf16[768,1024]{1,0:T(8,128)(2,1)} %get-tuple-element.27.up_grad_ref, ...), custom_call_target="tpu_custom_call" | custom-call | tf_op jit(solution)/shard_map/pallas_call | solution.py:374
  203.2 0.8 slice_multiply_fusion.2
  204.0 0.0 copy-done.5
  204.0 1.4 multiply_add_fusion.2
  205.4 0.0 copy-done.6
  205.4 0.6 add.63
  206.0 0.0 copy-done.3
  206.0 0.0 copy-done.4
  206.0 0.0 copy-start.1
  206.0 3.6 %multiply_add_fusion = (f32[256,1024]{1,0:T(8,128)}, f32[256,1024]{1,0:T(8,128)}) fusion(f32[256,1024]{1,0:T(8,128)S(1)} %copy-done.3, f32[256,1024]{1,0:T(8,128)} %get-tuple-element.18, f32[256,1024]{1,0:T(8,128)S(1)} %copy-done.4, f32[256,1024]{1,0:T(8,128)} %get-tuple-element.17), kind=kLoop, calls=%fused_computation.34 | loop fusion | flops 1048576 | bytes 6291456 | tf_op jit(solution)/shard_map/add | solution.py:674
  209.6 0.0 copy-done.1
  209.6 1.7 copy.18
Async XLA Ops:
  79.1 2.8 %copy-start = (bf16[2,768,1024]{2,1,0:T(8,128)(2,1)S(1)}, bf16[2,768,1024]{2,1,0:T(8,128)(2,1)}, u32[]{:S(2)}) copy-start(bf16[2,768,1024]{2,1,0:T(8,128)(2,1)} %get-tuple-element.13) | copy-start | bytes 9437188
  84.0 0.7 copy-start.7
  89.4 4.2 %copy-start.2 = (bf16[768,1024]{1,0:T(8,128)(2,1)S(1)}, bf16[768,1024]{1,0:T(8,128)(2,1)}, u32[]{:S(2)}) copy-start(bf16[768,1024]{1,0:T(8,128)(2,1)} %param.13) | copy-start | bytes 4718596
  109.5 94.5 %copy-start.5 = (f32[3,1024]{1,0:T(4,128)S(1)}, f32[3,1024]{1,0:T(4,128)}, u32[]{:S(2)}) copy-start(f32[3,1024]{1,0:T(4,128)} %param.20) | copy-start | bytes 36868
  109.5 95.9 %copy-start.6 = (f32[1024]{0:T(1024)S(1)}, f32[1024]{0:T(1024)}, u32[]{:S(2)}) copy-start(f32[1024]{0:T(1024)} %param.21) | copy-start | bytes 12292
  109.5 96.5 %copy-start.3 = (f32[256,1024]{1,0:T(8,128)S(1)}, f32[256,1024]{1,0:T(8,128)}, u32[]{:S(2)}) copy-start(f32[256,1024]{1,0:T(8,128)} %param.19) | copy-start | bytes 3145732
  109.5 96.5 %copy-start.4 = (f32[256,1024]{1,0:T(8,128)S(1)}, f32[256,1024]{1,0:T(8,128)}, u32[]{:S(2)}) copy-start(f32[256,1024]{1,0:T(8,128)} %param.18) | copy-start | bytes 3145732
  206.0 3.6 %copy-start.1 = (bf16[2,2,2,96,2048]{4,3,2,1,0:T(8,128)(2,1)S(1)}, bf16[2,2,2,96,2048]{4,3,2,1,0:T(8,128)(2,1)}, u32[]{:S(2)}) copy-start(bf16[2,2,2,96,2048]{4,3,2,1,0:T(8,128)(2,1)} %get-tuple-element.16) | copy-start | bytes 9437188

commit v4 on v3

--- a/solution.py
+++ b/solution.py
@@ -405,32 +405,6 @@
     return gate_sum, up_sum, rows.reshape(tokens, model), small_sum
 
 
-def shift_down(values, distance):
-    total_len = values.shape[1]
-    return jnp.pad(values, ((0, 0), (distance, 0), (0, 0)))[:, :total_len]
-
-
-def shift_up(values, distance):
-    return jnp.pad(values, ((0, 0), (0, distance), (0, 0)))[:, distance:]
-
-
-def causal_mix(pre_values, conv_taps, conv_bias):
-    return (
-        conv_taps[0] * shift_down(pre_values, 2)
-        + conv_taps[1] * shift_down(pre_values, 1)
-        + conv_taps[2] * pre_values
-        + conv_bias
-    )
-
-
-def mix_adjoint(mixed_grad, conv_taps):
-    return (
-        conv_taps[2] * mixed_grad
-        + conv_taps[1] * shift_up(mixed_grad, 1)
-        + conv_taps[0] * shift_up(mixed_grad, 2)
-    )
-
-
 def contract_last(left, right):
     return lax.dot_general(
         left, right, (((1,), (1,)), ((), ())), preferred_element_type=jnp.float32
@@ -625,6 +599,74 @@
     return weights.reshape(2, -1, width), gate_pre, up_value
 
 
+def middle_kernel(
+    gate_ref, up_ref, cotangent_ref, taps_ref, bias_ref, hidden_out, up_out, gate_out, small_out
+):
+    rows, width = cotangent_ref.shape
+    count = taps_ref.shape[0]
+    index = lax.broadcasted_iota(jnp.int32, (rows, width), 0)
+
+    def down(values, distance):
+        if distance == 0:
+            return values
+        return jnp.where(index >= distance, pltpu.roll(values, distance, 0), 0.0)
+
+    def up(values, distance):
+        if distance == 0:
+            return values
+        moved = pltpu.roll(values, rows - distance, 0)
+        return jnp.where(index < rows - distance, moved, 0.0)
+
+    taps = [taps_ref[k : k + 1, :] for k in range(count)]
+    for micro in range(2):
+        gate = gate_ref[micro].astype(jnp.float32)
+        value = up_ref[micro].astype(jnp.float32)
+        shifted = [down(gate, count - 1 - k) for k in range(count)]
+        mixed = bias_ref[...] + taps[0] * shifted[0]
+        for k in range(1, count):
+            mixed += taps[k] * shifted[k]
+        sig = jax.nn.sigmoid(mixed)
+        activated = mixed * sig
+        if micro == 0:
+            hidden_out[...] = (activated * value).astype(hidden_out.dtype)
+            continue
+        cotangent = cotangent_ref[...].astype(jnp.float32)
+        up_out[...] = (cotangent * activated).astype(up_out.dtype)
+        mixed_grad = cotangent * value * sig * (1.0 + mixed * (1.0 - sig))
+        total = taps[count - 1] * mixed_grad
+        for k in range(count - 1):
+            total += taps[k] * up(mixed_grad, count - 1 - k)
+        gate_out[...] = total.astype(gate_out.dtype)
+        small_out[...] = jnp.zeros_like(small_out)
+        for k in range(count):
+            small_out[k : k + 1, :] = jnp.sum(mixed_grad * shifted[k], axis=0, keepdims=True)
+        small_out[count : count + 1, :] = jnp.sum(mixed_grad, axis=0, keepdims=True)
+
+
+def middle(gate_pre, up_value, out_cotangent, conv_taps, conv_bias):
+    rows, width = out_cotangent.shape
+    count = conv_taps.shape[0]
+    small_rows = count + 1 + -(count + 1) % 8
+    block = math.gcd(width, 128)
+
+    def columns(height):
+        return pl.BlockSpec((height, block), lambda i: (0, i))
+
+    pair = pl.BlockSpec((2, rows, block), lambda i: (0, 0, i))
+    return pl.pallas_call(
+        middle_kernel,
+        grid=(width // block,),
+        out_shape=(
+            jax.ShapeDtypeStruct((rows, width), jnp.bfloat16),
+            jax.ShapeDtypeStruct((rows, width), jnp.bfloat16),
+            jax.ShapeDtypeStruct((rows, width), jnp.bfloat16),
+            jax.ShapeDtypeStruct((small_rows, width), jnp.float32),
+        ),
+        in_specs=[pair, pair, columns(rows), columns(count), columns(1)],
+        out_specs=(columns(rows), columns(rows), columns(rows), columns(small_rows)),
+    )(gate_pre, up_value, out_cotangent, conv_taps, conv_bias[None])
+
+
 def on_device(
     rows_later,
     rows_earlier,
@@ -640,32 +682,11 @@
 ):
     seq_len = rows_later.shape[0]
     pieces, gate_pre, up_value = gather_multiply(rows_later, rows_earlier, gate_proj, up_proj)
-    gate_float = gate_pre.astype(jnp.float32)
-    up_float = up_value.astype(jnp.float32)
-    mixed = causal_mix(gate_float, conv_taps, conv_bias)
-    sig_all = jax.nn.sigmoid(mixed)
-    activated = mixed * sig_all
-    hidden = (activated * up_float).astype(jnp.bfloat16)
-    hidden_later = hidden[0]
     grad_scale = lax.rsqrt(jnp.asarray(seq_len * lax.axis_size("fs"), jnp.float32))
-
-    cotangent = out_cotangent.astype(jnp.float32)[None]
-    mixed_back = mixed[1:]
-    sig_back = sig_all[1:]
-    up_grad = (cotangent * activated[1:]).astype(jnp.bfloat16)[0]
-    mixed_grad = cotangent * up_float[1:] * sig_back * (1.0 + mixed_back * (1.0 - sig_back))
-    gate_grad = mix_adjoint(mixed_grad, conv_taps).astype(jnp.bfloat16)[0]
-    gate_back = gate_float[1:]
-    tap_local = jnp.stack(
-        [
-            jnp.sum(mixed_grad * shift_down(gate_back, 2 - tap_index), axis=(0, 1))
-            for tap_index in range(conv_taps.shape[0])
-        ]
+    hidden_later, up_grad, gate_grad, small = middle(
+        gate_pre, up_value, out_cotangent, conv_taps, conv_bias
     )
-    bias_local = jnp.sum(mixed_grad, axis=(0, 1))
     taps = conv_taps.shape[0]
-    small = jnp.concatenate([tap_local, bias_local[None]], axis=0)
-    small = jnp.pad(small, ((0, -(taps + 1) % 8), (0, 0)))
     gate_summed, up_summed, input_grad, small_sum = reduce_all(
         rows_earlier, gate_grad, up_grad, pieces, small
     )

time: 213 us -> 191 us (0.90)
  other arithmetic: 34.5 us -> 6.35 us
  Pallas kernels: 171 us -> 181 us
  local copies, waits for them, and re-layouts: 4.66 us -> 1.69 us
    squeeze x2 -> x0, other arithmetic: 15.3 us -> none  [the longest x1 9.1 us: on_device(): up_grad = (cotangent * activated[1:]).astype(jnp.bfloat16)[0]]
    pallas_call x0 -> x1, Pallas kernels: none -> 9.82 us  [middle(): pl.pallas_call(middle_kernel, grid=(width // block,), out_shape=(jax.Shap...]
    div x1 -> x0, other arithmetic: 4.64 us -> none  [on_device(): sig_all = jax.nn.sigmoid(mixed)]
    mul x1 -> x0, other arithmetic: 4.19 us -> none  [on_device(): activated = mixed * sig_all]
    convert_element_type x2 -> x0, other arithmetic: 3.47 us -> none  [the longest x1 2.76 us: on_device(): up_float = up_value.astype(jnp.float32)]
    slice x2 -> x0, local copies, waits for them, and re-layouts: 2.9 us -> none  [the longest x1 2.06 us: on_device(): gate_back = gate_float[1:]]
where the time goes in v4:
time: 191 us; the launch traced here: 190 us
  Pallas kernels  181 us (95%)
  other arithmetic  6.35 us (3%)
    pallas_call x1, Pallas kernels, reduce_all(): pl.pallas_call(functools.partial(reduce_kernel, chips, side), out_shape=(...  93.5 us
    pallas_call x1, Pallas kernels, gather_multiply(): pl.pallas_call(functools.partial(gather_kernel, chips), out_shape=(jax.Sh...  77.6 us
    pallas_call x1, Pallas kernels, middle(): pl.pallas_call(middle_kernel, grid=(width // block,), out_shape=(jax.Shap...  9.82 us

profile of v4, /device:TPU:16, one launch (start us, length us, event | category | flops | bytes accessed | tf_op | source)
XLA Modules:
  0.0 189.7 jit_solution(18250954478440525171)
XLA Ops:
  0.6 77.6 %shard_map.154 = (bf16[2,4,512,1024]{3,2,1,0:T(8,128)(2,1)}, bf16[2,768,1024]{2,1,0:T(8,128)(2,1)}, bf16[2,768,1024]{2,1,0:T(8,128)(2,1)}) custom-call(bf16[768,2048]{1,0:T(8,128)(2,1)} %later_ref.1, bf16[768,2048]{1,0:T(8,128)(2,1)} %earlier_ref.3, bf16[256,1024]{1,0:T(8,128)(2,1)} %gate_ref.1, bf16[256,1024]{1,0:T(8,128)(2,1)} %up_ref.1), custom_call_target="tpu_custom_call" | custom-call | tf_op jit(solution)/shard_map/pallas_call | solution.py:578
  78.2 9.8 %shard_map.155 = (bf16[768,1024]{1,0:T(8,128)(2,1)}, bf16[768,1024]{1,0:T(8,128)(2,1)}, bf16[768,1024]{1,0:T(8,128)(2,1)}, f32[8,1024]{1,0:T(8,128)}) custom-call(bf16[2,768,1024]{2,1,0:T(8,128)(2,1)} %get-tuple-element.17.gate_ref, bf16[2,768,1024]{2,1,0:T(8,128)(2,1)} %get-tuple-element.18.up_ref, bf16[768,1024]{1,0:T(8,128)(2,1)} %cotangent_ref.1, ...), custom_call_target="tpu_custom_call" | custom-call | tf_op jit(solution)/shard_map/pallas_call | solution.py:656
  88.1 0.0 copy-start.3
  88.1 0.0 copy-start.4
  88.1 0.0 copy-start.1
  88.1 0.0 copy-start.2
  88.1 93.5 %shard_map.156 = (f32[256,1024]{1,0:T(8,128)}, f32[256,1024]{1,0:T(8,128)}, bf16[2,2,2,96,2048]{4,3,2,1,0:T(8,128)(2,1)}, f32[8,1024]{1,0:T(8,128)}) custom-call(bf16[768,2048]{1,0:T(8,128)(2,1)} %earlier_ref.3, bf16[768,1024]{1,0:T(8,128)(2,1)} %get-tuple-element.20.gate_grad_ref, bf16[768,1024]{1,0:T(8,128)(2,1)} %get-tuple-element.21.up_grad_ref, ...), custom_call_target="tpu_custom_call" | custom-call | tf_op jit(solution)/shard_map/pallas_call | solution.py:374
  181.6 0.8 slice_multiply_fusion
  182.4 0.0 copy-done.3
  182.4 1.4 multiply_add_fusion.2
  183.8 0.0 copy-done.4
  183.8 0.6 add.15
  184.4 0.0 copy-done.1
  184.4 0.0 copy-done.2
  184.4 0.0 copy-start
  184.4 3.6 %multiply_add_fusion = (f32[256,1024]{1,0:T(8,128)}, f32[256,1024]{1,0:T(8,128)}) fusion(f32[256,1024]{1,0:T(8,128)S(1)} %copy-done.1, f32[256,1024]{1,0:T(8,128)} %get-tuple-element.26, f32[256,1024]{1,0:T(8,128)S(1)} %copy-done.2, f32[256,1024]{1,0:T(8,128)} %get-tuple-element.25), kind=kLoop, calls=%fused_computation | loop fusion | flops 1048576 | bytes 6291456 | tf_op jit(solution)/shard_map/add | solution.py:695
  188.0 0.0 copy-done
  188.0 1.7 copy.18
Async XLA Ops:
  88.1 94.3 %copy-start.3 = (f32[3,1024]{1,0:T(4,128)S(1)}, f32[3,1024]{1,0:T(4,128)}, u32[]{:S(2)}) copy-start(f32[3,1024]{1,0:T(4,128)} %param.20) | copy-start | bytes 36868
  88.1 95.7 %copy-start.4 = (f32[1024]{0:T(1024)S(1)}, f32[1024]{0:T(1024)}, u32[]{:S(2)}) copy-start(f32[1024]{0:T(1024)} %param.21) | copy-start | bytes 12292
  88.1 96.3 %copy-start.1 = (f32[256,1024]{1,0:T(8,128)S(1)}, f32[256,1024]{1,0:T(8,128)}, u32[]{:S(2)}) copy-start(f32[256,1024]{1,0:T(8,128)} %param.19) | copy-start | bytes 3145732
  88.1 96.3 %copy-start.2 = (f32[256,1024]{1,0:T(8,128)S(1)}, f32[256,1024]{1,0:T(8,128)}, u32[]{:S(2)}) copy-start(f32[256,1024]{1,0:T(8,128)} %param.18) | copy-start | bytes 3145732
  184.4 3.6 %copy-start = (bf16[2,2,2,96,2048]{4,3,2,1,0:T(8,128)(2,1)S(1)}, bf16[2,2,2,96,2048]{4,3,2,1,0:T(8,128)(2,1)}, u32[]{:S(2)}) copy-start(bf16[2,2,2,96,2048]{4,3,2,1,0:T(8,128)(2,1)} %get-tuple-element.24) | copy-start | bytes 9437188
